TPU v7x, 768 devices: a whole 4x8x12 slice. The times are simulated.
768 devices in a mesh: ep: 24 (over z, core), tp: 32 (over y, x).
Axes of the slice: x: 4, y: 8, z: 12, core: 2. Of those that a mesh axis runs over, the one named last changes fastest.
Arguments:
- tokens: bfloat16 [768, 2560], P('ep'), may hold values from -6 to 6
- norm_gain: float32 [2560], replicated, may hold values from 0.1 to 1.9
- route: int32 [768, 4], P('ep'), may hold values from 0 to 23, all different within a row; in each aligned block of 32 rows (0 to 31, 32 to 63, ...) at most 8 rows name the same one
- route_weight: float32 [768, 4], P('ep'), may hold values from 0.1 to 1
- gate_weight: bfloat16 [24, 8960, 2560], P('ep', 'tp'), may hold values from -0.125 to 0.125
- up_weight: bfloat16 [24, 8960, 2560], P('ep', 'tp'), may hold values from -0.125 to 0.125
- down_weight: bfloat16 [24, 8960, 2560], P('ep', 'tp'), may hold values from -0.0625 to 0.0625
Outputs:
- mixed: bfloat16 [768, 2560], P('ep', 'tp')
Inputs may be any that keep to these rules, and one draw needn't show every extreme that they name: `route`: each row names 4 different experts. Among the rows of one index of ep no expert is named more than 8 times, a bound that some block reaches.
All inputs are finite; a program needn't handle non-finite values.
Results may differ from a plain program's by a relative error of at most 0.018.
Values may be sent and summed in bfloat16 or wider, within the bound.
No kernel may reach another device: no remote copies, remote signals or barrier semaphores. Data moves between devices by JAX's collectives and lax.ppermute only.
A program may use at most 64 MiB of HBM per device.

v0:
```python
import jax
import jax.numpy as jnp
from jax import lax
from jax.sharding import PartitionSpec as P

epsilon = 1e-06


def split_up(shard, dim, size):
    lengths = shard.shape
    tiles = shard.reshape(*lengths[:dim], size, lengths[dim] // size, *lengths[dim + 1 :])
    return jnp.moveaxis(tiles, dim, 0)


def sent_and_summed(shard, axis, dim):
    size = lax.axis_size(axis)
    tiles = lax.all_to_all(split_up(shard, dim, size), axis, 0, 0, tiled=True)
    return jnp.sum(tiles.astype(jnp.float32), axis=0)


def on_device(tokens, norm_gain, route, route_weight, gate_weight, up_weight, down_weight):
    tok_rows, width = tokens.shape
    top_count = route.shape[1]
    local_experts = gate_weight.shape[0]
    ep_count = lax.axis_size("ep")
    tp_count = lax.axis_size("tp")
    experts = local_experts * ep_count
    capacity = min(tok_rows, max(2, (3 * tok_rows * top_count + 2 * experts - 1) // (2 * experts)))
    width_share = width // tp_count
    values = tokens.astype(jnp.float32)
    scaled = values * lax.rsqrt(jnp.mean(values * values, axis=-1, keepdims=True) + epsilon)
    normed = (scaled * norm_gain).astype(jnp.bfloat16)
    flat_route = route.reshape(tok_rows * top_count)
    onehot = (flat_route[:, None] == jnp.arange(experts, dtype=jnp.int32)[None, :]).astype(
        jnp.int32
    )
    slot_number = jnp.sum((jnp.cumsum(onehot, axis=0) - 1) * onehot, axis=-1)
    slot_index = flat_route * capacity + slot_number
    placing = (
        slot_index[None, :] == jnp.arange(experts * capacity, dtype=jnp.int32)[:, None]
    ).astype(jnp.bfloat16)
    repeated = jnp.repeat(normed, top_count, axis=0)
    send = jnp.dot(placing, repeated, preferred_element_type=jnp.float32).astype(jnp.bfloat16)
    send = send.reshape(ep_count, local_experts, capacity, width)
    arrived = lax.all_to_all(send, "ep", split_axis=0, concat_axis=0, tiled=True)
    gate = jnp.einsum("sjcd,jfd->sjcf", arrived, gate_weight, preferred_element_type=jnp.float32)
    upward = jnp.einsum("sjcd,jfd->sjcf", arrived, up_weight, preferred_element_type=jnp.float32)
    hidden = (jax.nn.silu(gate) * upward).astype(jnp.bfloat16)
    partial_value = jnp.einsum(
        "sjcf,jfd->sjcd", hidden, down_weight, preferred_element_type=jnp.float32
    )
    shares = sent_and_summed(partial_value.astype(jnp.bfloat16), "tp", 3).astype(jnp.bfloat16)
    returned = lax.all_to_all(shares, "ep", split_axis=0, concat_axis=0, tiled=True)
    results = returned.reshape(experts * capacity, width_share)
    picked = results[slot_index].reshape(tok_rows, top_count, width_share).astype(jnp.float32)
    mixed = jnp.sum(route_weight[:, :, None] * picked, axis=1)
    return mixed.astype(jnp.bfloat16)


def solution(mesh):
    placed = (
        P("ep", None),
        P(),
        P("ep", None),
        P("ep", None),
        P("ep", "tp", None),
        P("ep", "tp", None),
        P("ep", "tp", None),
    )
    return jax.shard_map(
        on_device, mesh=mesh, in_specs=placed, out_specs=P("ep", "tp"), check_vma=False
    )
```

profile of v0, /device:TPU:1, one launch (start us, length us, event | category | flops | bytes accessed | tf_op | source)
XLA Modules:
  0.0 135.5 jit_solution(13566480292003826512)
XLA Ops:
  0.0 0.9 copy.15
  0.9 0.1 reshape.86
  1.0 0.1 fusion.38
  1.1 0.2 reduce_window_sum.11
  1.3 0.2 select_reduce_fusion
  1.4 1.1 fusion.28
  2.5 1.0 fusion.30
  3.5 0.2 broadcast_in_dim.2
  3.7 0.1 reshape.87
  3.9 0.4 fusion.1
  4.3 55.6 %all_to_all.15 = bf16[24,1,8,2560]{3,2,1,0:T(8,128)(2,1)S(1)} all-to-all(bf16[24,1,8,2560]{3,2,1,0:T(8,128)(2,1)S(1)} %fusion.1), channel_id=1, replica_groups=mesh['ep'=24,'tp'=32] {'ep'}, dimensions={0} | all-to-all | bytes 1966080 | tf_op jit(solution)/shard_map/all_to_all | solution.py:45
  59.9 0.8 fusion.7
  60.7 3.9 %fusion = bf16[24,1,8,2560]{3,2,0,1:T(8,128)(2,1)} fusion(bf16[1,280,2560]{2,1,0:T(8,128)(2,1)S(1)} %copy-done, bf16[1,280,2560]{2,1,0:T(8,128)(2,1)} %param.12, bf16[24,1,8,2560]{3,2,1,0:T(8,128)(2,1)S(1)} %all_to_all.15, f32[24,1,8,280]{3,2,0,1:T(8,128)S(1)} %fusion.7), kind=kOutput, calls=%fused_computation.3 | convolution fusion | flops 551316480 | bytes 5048320 | tf_op jit(solution)/shard_map/sjcf,jfd->sjcd/dot_general | solution.py:49
  64.6 3.1 %reshape.94 = bf16[24,1,8,32,80]{4,3,2,0,1:T(8,128)(2,1)S(1)} reshape(bf16[24,1,8,2560]{3,2,0,1:T(8,128)(2,1)} %fusion) | data formatting | bytes 1966080 | tf_op jit(solution)/shard_map/reshape | solution.py:11
  67.7 1.8 %copy.20 = bf16[24,1,8,32,80]{4,2,0,1,3:T(8,128)(2,1)} copy(bf16[24,1,8,32,80]{4,3,2,0,1:T(8,128)(2,1)S(1)} %reshape.94) | data formatting | bytes 1966080 | tf_op jit(solution)/shard_map/reshape | solution.py:11
  69.4 9.8 %all-to-all-start.1 = ((bf16[32,24,1,8,80]{4,3,1,2,0:T(8,128)(2,1)}), bf16[32,24,1,8,80]{4,3,1,2,0:T(8,128)(2,1)S(1)}, u32[]{:S(2)}, u32[]{:S(2)}) async-start(bf16[32,24,1,8,80]{4,3,1,2,0:T(8,128)(2,1)} %bitcast.83), calls=%async_computation.1 | async-start | bytes 3145728 | tf_op jit(solution)/shard_map/all_to_all | solution.py:17
  79.2 0.1 copy.18
  79.3 0.1 mul.74
  79.5 36.1 %all-to-all-done.1 = bf16[32,24,1,8,80]{4,3,1,2,0:T(8,128)(2,1)S(1)} async-done(((bf16[32,24,1,8,80]{4,3,1,2,0:T(8,128)(2,1)}), bf16[32,24,1,8,80]{4,3,1,2,0:T(8,128)(2,1)S(1)}, u32[]{:S(2)}, u32[]{:S(2)}) %all-to-all-start.1) | async-done | bytes 983072 | tf_op jit(solution)/shard_map/all_to_all | solution.py:17
  115.6 1.0 reduce_sum.45
  116.6 7.2 %all-to-all-start.2 = ((bf16[24,1,8,80]{3,2,1,0:T(8,128)(2,1)}), bf16[24,1,8,80]{3,2,1,0:T(8,128)(2,1)S(1)}, u32[]{:S(2)}, u32[]{:S(2)}) async-start(bf16[24,1,8,80]{3,2,1,0:T(8,128)(2,1)} %bitcast.22), calls=%async_computation.2 | async-start | bytes 98304 | tf_op jit(solution)/shard_map/all_to_all | solution.py:53
  123.8 10.2 %all-to-all-done.2 = bf16[24,1,8,80]{3,2,1,0:T(8,128)(2,1)S(1)} async-done(((bf16[24,1,8,80]{3,2,1,0:T(8,128)(2,1)}), bf16[24,1,8,80]{3,2,1,0:T(8,128)(2,1)S(1)}, u32[]{:S(2)}, u32[]{:S(2)}) %all-to-all-start.2) | async-done | bytes 30752 | tf_op jit(solution)/shard_map/all_to_all | solution.py:53
  134.0 0.7 gather_fusion
  134.7 0.7 fusion.37
  (14 shorter events, 0.1 us)
Async XLA Ops:
  0.0 60.7 %copy-start = (bf16[1,280,2560]{2,1,0:T(8,128)(2,1)S(1)}, bf16[1,280,2560]{2,1,0:T(8,128)(2,1)}, u32[]{:S(2)}) copy-start(bf16[1,280,2560]{2,1,0:T(8,128)(2,1)} %param.13) | copy-start | bytes 4300804
  3.9 56.0 %copy-start.1 = (bf16[1,280,2560]{2,1,0:T(8,128)(2,1)S(1)}, bf16[1,280,2560]{2,1,0:T(8,128)(2,1)}, u32[]{:S(2)}) copy-start(bf16[1,280,2560]{2,1,0:T(8,128)(2,1)} %param.11) | copy-start | bytes 4300804
  69.4 9.8 %copy-start.2 = (s32[32,4]{0,1:T(4,128)S(1)}, s32[32,4]{0,1:T(4,128)}, u32[]{:S(2)}) copy-start(s32[32,4]{0,1:T(4,128)} %param.9) | copy-start | bytes 1540
  69.4 10.0 %copy-start.3 = (f32[32,4]{0,1:T(4,128)S(1)}, f32[32,4]{0,1:T(4,128)}, u32[]{:S(2)}) copy-start(f32[32,4]{0,1:T(4,128)} %param.10) | copy-start | bytes 1540
  69.4 46.2 %all-to-all-start.1 = ((bf16[32,24,1,8,80]{4,3,1,2,0:T(8,128)(2,1)}), bf16[32,24,1,8,80]{4,3,1,2,0:T(8,128)(2,1)S(1)}, u32[]{:S(2)}, u32[]{:S(2)}) async-start(bf16[32,24,1,8,80]{4,3,1,2,0:T(8,128)(2,1)} %bitcast.83), calls=%async_computation.1 | async-start | bytes 3145728 | tf_op jit(solution)/shard_map/all_to_all | solution.py:17
  116.6 17.5 %all-to-all-start.2 = ((bf16[24,1,8,80]{3,2,1,0:T(8,128)(2,1)}), bf16[24,1,8,80]{3,2,1,0:T(8,128)(2,1)S(1)}, u32[]{:S(2)}, u32[]{:S(2)}) async-start(bf16[24,1,8,80]{3,2,1,0:T(8,128)(2,1)} %bitcast.22), calls=%async_computation.2 | async-start | bytes 98304 | tf_op jit(solution)/shard_map/all_to_all | solution.py:53
where the time goes:
time: 136 us; the launch traced here: 135 us
  blocking collectives  55.6 us (41%)
  waiting for transfers between devices  46.3 us (34%)
  starting transfers between devices  17 us (12%)
  local copies, waits for them, and re-layouts  7.15 us (5%)
  matrix products  5.09 us (4%)
  other arithmetic  4.23 us (3%)
    all_to_all x1, blocking collectives, on_device(): lax.all_to_all(send, 'ep', split_axis=0, concat_axis=0, tiled=True)  55.6 us
    all_to_all x1, waiting for transfers between devices, sent_and_summed(): tiles = lax.all_to_all(split_up(shard, dim, size), axis, 0, 0, tiled=True)  36.1 us
    all_to_all x1, waiting for transfers between devices, on_device(): lax.all_to_all(shares, 'ep', split_axis=0, concat_axis=0, tiled=True)  10.2 us
    all_to_all x1, starting transfers between devices, sent_and_summed(): tiles = lax.all_to_all(split_up(shard, dim, size), axis, 0, 0, tiled=True)  9.79 us
    all_to_all x1, starting transfers between devices, on_device(): lax.all_to_all(shares, 'ep', split_axis=0, concat_axis=0, tiled=True)  7.19 us
    reshape x2, local copies, waits for them, and re-layouts, split_up(): shard.reshape(*lengths[:dim], size, lengths[dim] // size, *lengths[dim +...  4.85 us
    dot_general x1, matrix products, on_device(): jnp.einsum('sjcf,jfd->sjcd', hidden, down_weight, preferred_element_type=...  3.89 us
  transfers between devices with their start and end apart: 2, of which 2 were waited for; matrix products, arithmetic and copies ran while one was open for 0% of the time, Pallas kernels for 0%

commit v1 on v0

v1 whole, which is shorter than its diff:
```python
import jax
import jax.numpy as jnp
from jax import lax
from jax.experimental import pallas as pl
from jax.experimental.pallas import tpu as pltpu
from jax.sharding import Mesh
from jax.sharding import PartitionSpec as P

epsilon = 1e-06
bf16 = jnp.bfloat16
f32 = jnp.float32

Z, C, Y, X = 12, 2, 8, 4
EP = Z * C
TP = Y * X


def whole_vmem(count):
    return [pl.BlockSpec(memory_space=pltpu.VMEM)] * count


def slots_of(route_t, experts, rows):
    expert = lax.broadcasted_iota(jnp.int32, (experts, rows), 0)
    named = jnp.zeros((experts, rows), f32)
    for k in range(route_t.shape[0]):
        named = named + (route_t[k : k + 1, :] == expert).astype(f32)
    before = lax.broadcasted_iota(jnp.int32, (rows, rows), 0) < lax.broadcasted_iota(
        jnp.int32, (rows, rows), 1
    )
    earlier = jnp.dot(named, before.astype(f32), preferred_element_type=f32)
    return named, earlier


def place_kernel(at_ref, tokens_ref, gain_ref, route_ref, send_ref):
    rows, width = tokens_ref.shape
    experts, cap, share = EP, send_ref.shape[0] // EP, send_ref.shape[1]
    values = tokens_ref[...].astype(f32)
    scale = lax.rsqrt(jnp.mean(values * values, axis=-1, keepdims=True) + epsilon)
    start = pl.multiple_of(at_ref[0] * share, 128)
    own = tokens_ref[:, pl.ds(start, share)].astype(f32)
    normed = (own * scale * gain_ref[:, pl.ds(start, share)]).astype(bf16)
    named, earlier = slots_of(route_ref[...], experts, rows)
    spots = experts * cap
    spot = lax.broadcasted_iota(jnp.int32, (spots, experts), 0)
    spread = (spot // cap == lax.broadcasted_iota(jnp.int32, (spots, experts), 1)).astype(f32)
    hit = jnp.dot(spread, named, preferred_element_type=f32)
    count = jnp.dot(spread, earlier, preferred_element_type=f32)
    slot = (lax.broadcasted_iota(jnp.int32, (spots, rows), 0) % cap).astype(f32)
    placing = jnp.where(count == slot, hit, 0.0).astype(bf16)
    send_ref[...] = jnp.dot(placing, normed, preferred_element_type=f32).astype(bf16)


def expert_kernel(rows_ref, gate_ref, up_ref, down_ref, out_ref):
    parts, _, share = rows_ref.shape
    contract = (((1,), (1,)), ((), ()))
    gate = up = None
    for p in range(parts):
        rows = rows_ref[p]
        cols = slice(p * share, (p + 1) * share)
        g = lax.dot_general(rows, gate_ref[:, cols], contract, preferred_element_type=f32)
        u = lax.dot_general(rows, up_ref[:, cols], contract, preferred_element_type=f32)
        gate = g if gate is None else gate + g
        up = u if up is None else up + u
    hidden = (gate / (1.0 + jnp.exp(-gate)) * up).astype(bf16)
    block = share // Y
    sums = jnp.dot(hidden, down_ref[...], preferred_element_type=f32).astype(bf16)
    for p in range(parts):
        blocks = [sums[:, (y * X + p) * block : (y * X + p + 1) * block] for y in range(Y)]
        out_ref[p] = jnp.concatenate(blocks, axis=1)


def sum_x_kernel(in_ref, out_ref):
    total = in_ref[0].astype(f32)
    for p in range(1, in_ref.shape[0]):
        total = total + in_ref[p].astype(f32)
    total = total.astype(bf16)
    share = out_ref.shape[2]
    for p in range(out_ref.shape[0]):
        out_ref[p] = total[:, p * share : (p + 1) * share]


def sum_y_kernel(in_ref, out_ref):
    total = in_ref[0].astype(f32)
    for p in range(1, in_ref.shape[0]):
        total = total + in_ref[p].astype(f32)
    out_ref[...] = total.astype(bf16)


def mix_kernel(got_ref, route_ref, weight_ref, out_ref):
    rows = out_ref.shape[0]
    spots = got_ref.shape[0]
    experts, cap = EP, spots // EP
    route_t = route_ref[...]
    named, earlier = slots_of(route_t, experts, rows)
    expert = lax.broadcasted_iota(jnp.int32, (experts, rows), 0)
    weight = jnp.zeros((experts, rows), f32)
    for k in range(route_t.shape[0]):
        weight = weight + jnp.where(route_t[k : k + 1, :] == expert, weight_ref[k : k + 1, :], 0.0)
    spot = lax.broadcasted_iota(jnp.int32, (spots, experts), 0)
    spread = (spot // cap == lax.broadcasted_iota(jnp.int32, (spots, experts), 1)).astype(f32)
    exact = lax.Precision.HIGHEST
    count = jnp.dot(spread, earlier, preferred_element_type=f32)
    hit = jnp.dot(spread, weight, preferred_element_type=f32, precision=exact)
    slot = (lax.broadcasted_iota(jnp.int32, (spots, rows), 0) % cap).astype(f32)
    chosen = jnp.where(count == slot, hit, 0.0)
    mixed = lax.dot_general(
        chosen,
        got_ref[...].astype(f32),
        (((0,), (0,)), ((), ())),
        preferred_element_type=f32,
        precision=exact,
    )
    out_ref[...] = mixed.astype(bf16)


def on_device(tokens, norm_gain, route, route_weight, gate_weight, up_weight, down_weight):
    tok_rows, width = tokens.shape
    cap = 8
    quarter = width // X
    share = width // TP
    spots = EP * cap
    route_t = route.T
    weight_t = route_weight.T
    at = lax.axis_index("x").astype(jnp.int32).reshape(1)

    send = pl.pallas_call(
        place_kernel,
        in_specs=[pl.BlockSpec(memory_space=pltpu.SMEM)] + whole_vmem(3),
        out_specs=pl.BlockSpec(memory_space=pltpu.VMEM),
        out_shape=jax.ShapeDtypeStruct((spots, quarter), bf16),
        name="place",
    )(at, tokens, norm_gain.reshape(1, width), route_t)
    arrived = lax.all_to_all(send.reshape(EP, cap, quarter), ("z", "c"), 0, 0, tiled=True)
    rows = lax.all_gather(arrived.reshape(spots, quarter), "x", axis=0, tiled=False)
    part = pl.pallas_call(
        expert_kernel,
        in_specs=whole_vmem(4),
        out_specs=pl.BlockSpec(memory_space=pltpu.VMEM),
        out_shape=jax.ShapeDtypeStruct((X, spots, quarter), bf16),
        name="expert",
    )(rows, gate_weight[0], up_weight[0], down_weight[0])
    part = lax.all_to_all(part, "x", 0, 0, tiled=True)
    part = pl.pallas_call(
        sum_x_kernel,
        in_specs=whole_vmem(1),
        out_specs=pl.BlockSpec(memory_space=pltpu.VMEM),
        out_shape=jax.ShapeDtypeStruct((Y, spots, share), bf16),
        name="sum_x",
    )(part)
    part = lax.all_to_all(part, "y", 0, 0, tiled=True)
    done = pl.pallas_call(
        sum_y_kernel,
        in_specs=whole_vmem(1),
        out_specs=pl.BlockSpec(memory_space=pltpu.VMEM),
        out_shape=jax.ShapeDtypeStruct((spots, share), bf16),
        name="sum_y",
    )(part)
    back = lax.all_to_all(done.reshape(EP, cap, share), ("z", "c"), 0, 0, tiled=True)
    return pl.pallas_call(
        mix_kernel,
        in_specs=whole_vmem(3),
        out_specs=pl.BlockSpec(memory_space=pltpu.VMEM),
        out_shape=jax.ShapeDtypeStruct((tok_rows, share), bf16),
        name="mix",
    )(back.reshape(spots, share), route_t, weight_t)


def solution(mesh):
    fine = Mesh(mesh.devices.reshape(Z, C, Y, X), ("z", "c", "y", "x"))
    ep, tp = ("z", "c"), ("y", "x")
    placed = (
        P(ep, None),
        P(),
        P(ep, None),
        P(ep, None),
        P(ep, tp, None),
        P(ep, tp, None),
        P(ep, tp, None),
    )
    return jax.shard_map(
        on_device, mesh=fine, in_specs=placed, out_specs=P(ep, tp), check_vma=False
    )
```

time: 136 us -> 116 us (0.85)
  waiting for transfers between devices: 46.3 us -> 0 us
  blocking collectives: 55.6 us -> 97.9 us
  starting transfers between devices: 17 us -> 0 us
  Pallas kernels: 0 us -> 13.7 us
  matrix products: 5.09 us -> 0 us
  other arithmetic: 4.23 us -> 0 us
  local copies, waits for them, and re-layouts: 7.15 us -> 3.42 us
    all_to_all x2 -> x0, waiting for transfers between devices: 46.3 us -> none  [the longest x1 36.1 us: sent_and_summed(): tiles = lax.all_to_all(split_up(shard, dim, size), axis, 0, 0, tiled=True)]
    all_to_all x1 -> x4, blocking collectives: 55.6 us -> 83.8 us  [the longest x1 31.6 us: on_device(): lax.all_to_all(send.reshape(EP, cap, quarter), ('z', 'c'), 0, 0, tiled=True)]
    all_to_all x2 -> x0, starting transfers between devices: 17 us -> none  [the longest x1 9.79 us: sent_and_summed(): tiles = lax.all_to_all(split_up(shard, dim, size), axis, 0, 0, tiled=True)]
    all_gather x0 -> x1, blocking collectives: none -> 14.1 us  [on_device(): lax.all_gather(arrived.reshape(spots, quarter), 'x', axis=0, tiled=False)]
    pallas_call x0 -> x5, Pallas kernels: none -> 13.7 us  [the longest x1 5.78 us: on_device(): pl.pallas_call(expert_kernel, in_specs=whole_vmem(4), out_specs=pl.BlockS...]
    dot_general x3 -> x0, matrix products: 5.09 us -> none  [the longest x1 3.89 us: on_device(): jnp.einsum('sjcf,jfd->sjcd', hidden, down_weight, preferred_element_type=...]
    reshape x4 -> x1, local copies, waits for them, and re-layouts: 5.1 us -> 1.31 us  [on_device(): norm_gain.reshape(1, width)]
    reduce_sum x4 -> x0, other arithmetic: 2.9 us -> none  [the longest x1 1.06 us: on_device(): jnp.mean(values * values, axis=-1, keepdims=True) + epsilon]
  transfers between devices with their start and end apart: 2 -> 0, of which waited for: 2 -> 0; matrix products, arithmetic and copies ran while one was open for 0% -> 0% of each run, Pallas kernels for 0% -> 0%
where the time goes in v1:
time: 116 us; the launch traced here: 115 us
  blocking collectives  97.9 us (84%)
  Pallas kernels  13.7 us (12%)
  local copies, waits for them, and re-layouts  3.42 us (3%)
    all_to_all x1, blocking collectives, on_device(): lax.all_to_all(send.reshape(EP, cap, quarter), ('z', 'c'), 0, 0, tiled=True)  31.6 us
    all_to_all x1, blocking collectives, on_device(): lax.all_to_all(done.reshape(EP, cap, share), ('z', 'c'), 0, 0, tiled=True)  19.6 us
    all_to_all x1, blocking collectives, on_device(): part = lax.all_to_all(part, 'y', 0, 0, tiled=True)  16.8 us
    all_to_all x1, blocking collectives, on_device(): part = lax.all_to_all(part, 'x', 0, 0, tiled=True)  15.9 us
    all_gather x1, blocking collectives, on_device(): lax.all_gather(arrived.reshape(spots, quarter), 'x', axis=0, tiled=False)  14.1 us
    pallas_call x1, Pallas kernels, on_device(): pl.pallas_call(expert_kernel, in_specs=whole_vmem(4), out_specs=pl.BlockS...  5.78 us

profile of v1, /device:TPU:1, one launch (start us, length us, event | category | flops | bytes accessed | tf_op | source)
XLA Modules:
  0.0 115.1 jit_solution(294624648774375574)
XLA Ops:
  0.0 1.3 %reshape.16.gain_ref = f32[1,2560]{1,0:T(1,128)} reshape(f32[2560]{0:T(1024)} %param.8) | data formatting | bytes 20480 | tf_op jit(solution)/shard_map/reshape | solution.py:132
  1.3 2.1 %place.1 = bf16[192,640]{1,0:T(8,128)(2,1)} custom-call(s32[1]{0:T(128)} %bitcast.at_ref, bf16[32,2560]{1,0:T(8,128)(2,1)} %tokens_ref.1, f32[1,2560]{1,0:T(1,128)} %reshape.16.gain_ref, s32[4,32]{1,0:T(4,128)} %bitcast.17), custom_call_target="tpu_custom_call" | custom-call | tf_op jit(solution)/shard_map/place/pallas_call | solution.py:126
  3.4 31.6 %all_to_all.20 = bf16[24,8,640]{2,1,0:T(8,128)(2,1)S(1)} all-to-all(bf16[24,8,640]{2,1,0:T(8,128)(2,1)} %bitcast.14), channel_id=1, replica_groups=mesh['z'=12,'c'=2,'y'=8,'x'=4] {'z','c'}, dimensions={0} | all-to-all | bytes 491520 | tf_op jit(solution)/shard_map/all_to_all | solution.py:133
  35.0 14.1 %all_gather.3.rows_ref = bf16[4,192,640]{2,1,0:T(8,128)(2,1)} all-gather(bf16[1,192,640]{2,1,0:T(8,128)(2,1)S(1)} %bitcast.13), channel_id=1, replica_groups=mesh['z'=12,'c'=2,'y'=8,'x'=4] {'x'}, dimensions={0}, use_global_device_ids=true | all-gather | bytes 1228800 | tf_op jit(solution)/shard_map/all_gather | solution.py:134
  49.1 5.8 %expert.1 = bf16[4,192,640]{2,1,0:T(8,128)(2,1)} custom-call(bf16[4,192,640]{2,1,0:T(8,128)(2,1)} %all_gather.3.rows_ref, bf16[280,2560]{1,0:T(8,128)(2,1)} %bitcast.10, bf16[280,2560]{1,0:T(8,128)(2,1)} %bitcast.11, bf16[280,2560]{1,0:T(8,128)(2,1)} %bitcast.12), custom_call_target="tpu_custom_call" | custom-call | tf_op jit(solution)/shard_map/expert/pallas_call | solution.py:135
  54.9 15.9 %all_to_all.21.in_ref = bf16[4,192,640]{2,1,0:T(8,128)(2,1)} all-to-all(bf16[4,192,640]{2,1,0:T(8,128)(2,1)} %expert.1), channel_id=1, replica_groups=mesh['z'=12,'c'=2,'y'=8,'x'=4] {'x'}, dimensions={0} | all-to-all | bytes 1966080 | tf_op jit(solution)/shard_map/all_to_all | solution.py:142
  70.7 2.2 %sum_x.1 = bf16[8,192,80]{2,1,0:T(8,128)(2,1)} custom-call(bf16[4,192,640]{2,1,0:T(8,128)(2,1)} %all_to_all.21.in_ref), custom_call_target="tpu_custom_call" | custom-call | tf_op jit(solution)/shard_map/sum_x/pallas_call | solution.py:143
  72.9 1.2 %copy.8 = bf16[8,192,80]{1,2,0:T(8,128)(2,1)S(1)} copy(bf16[8,192,80]{2,1,0:T(8,128)(2,1)} %sum_x.1) | data formatting | bytes 491520 | tf_op jit(solution)/shard_map/sum_x/pallas_call | solution.py:143
  74.1 16.8 %all_to_all.22 = bf16[8,192,80]{1,2,0:T(8,128)(2,1)S(1)} all-to-all(bf16[8,192,80]{1,2,0:T(8,128)(2,1)S(1)} %copy.8), channel_id=1, replica_groups=mesh['z'=12,'c'=2,'y'=8,'x'=4] {'y'}, dimensions={0} | all-to-all | bytes 491520 | tf_op jit(solution)/shard_map/all_to_all | solution.py:150
  90.9 0.9 copy.9.in_ref
  91.8 1.7 %sum_y.1 = bf16[192,80]{1,0:T(8,128)(2,1)} custom-call(bf16[8,192,80]{2,1,0:T(8,128)(2,1)} %copy.9.in_ref), custom_call_target="tpu_custom_call" | custom-call | tf_op jit(solution)/shard_map/sum_y/pallas_call | solution.py:151
  93.5 19.6 %all_to_all.23 = bf16[24,8,80]{2,1,0:T(8,128)(2,1)} all-to-all(bf16[24,8,80]{2,1,0:T(8,128)(2,1)} %bitcast.15), channel_id=1, replica_groups=mesh['z'=12,'c'=2,'y'=8,'x'=4] {'z','c'}, dimensions={0} | all-to-all | bytes 61440 | tf_op jit(solution)/shard_map/all_to_all | solution.py:158
  113.0 2.0 %mix.1 = bf16[32,80]{1,0:T(8,128)(2,1)} custom-call(bf16[192,80]{1,0:T(8,128)(2,1)} %bitcast.16, s32[4,32]{1,0:T(4,128)} %bitcast.18, f32[4,32]{1,0:T(4,128)} %bitcast.19), custom_call_target="tpu_custom_call" | custom-call | tf_op jit(solution)/shard_map/mix/pallas_call | solution.py:159

commit v2 on v0

v2 whole, which is shorter than its diff:
```python
import jax
import jax.numpy as jnp
from jax import lax
from jax.experimental import pallas as pl
from jax.experimental.pallas import tpu as pltpu
from jax.sharding import Mesh
from jax.sharding import PartitionSpec as P

epsilon = 1e-06
bf16 = jnp.bfloat16
f32 = jnp.float32

Z, C, Y, X = 12, 2, 8, 4
EP = Z * C
TP = Y * X
CAP = 8
LANES = 128
SCOPED = 16 << 20
VMEM = pl.BlockSpec(memory_space=pltpu.VMEM)


HBM = pl.BlockSpec(memory_space=pl.ANY)


def near(array):
    return pltpu.with_memory_space_constraint(array, pltpu.VMEM)


def far(array):
    return pltpu.with_memory_space_constraint(array, pltpu.HBM)


def local(kernel, name, specs, outs, scratch=()):
    return pl.pallas_call(
        kernel,
        in_specs=specs,
        out_specs=tuple(VMEM for _ in outs) if isinstance(outs, tuple) else VMEM,
        out_shape=outs,
        scratch_shapes=scratch,
        compiler_params=pltpu.CompilerParams(vmem_limit_bytes=SCOPED),
        name=name,
    )


def summed(ref):
    total = ref[0].astype(f32)
    for p in range(1, ref.shape[0]):
        total = total + ref[p].astype(f32)
    return total


def per_slot(table):
    rows = table.shape[1]
    lines = [jnp.broadcast_to(table[e : e + 1, :], (CAP, rows)) for e in range(table.shape[0])]
    return jnp.concatenate(lines, axis=0)


def place_kernel(at_ref, *refs):
    sources, (send_ref, chosen_ref) = refs[:4], refs[4:6]
    (tokens_ref, gain_ref, route_ref, weight_ref), sems = refs[6:10], refs[10]
    copies = [
        pltpu.make_async_copy(source, there, sems.at[i])
        for i, (source, there) in enumerate(zip(sources, refs[6:10]))
    ]
    for copy in copies:
        copy.start()
    for copy in copies:
        copy.wait()
    rows = tokens_ref.shape[0]
    share = send_ref.shape[1]
    values = tokens_ref[...].astype(f32)
    scale = lax.rsqrt(jnp.mean(values * values, axis=-1, keepdims=True) + epsilon)
    start = pl.multiple_of(at_ref[0] * share, LANES)
    own = tokens_ref[:, pl.ds(start, share)].astype(f32)
    gain = gain_ref[pl.ds(start, share)].reshape(1, share)
    normed = (own * scale * gain).astype(bf16)
    expert = lax.broadcasted_iota(jnp.int32, (EP, rows), 0)
    named = jnp.zeros((EP, rows), f32)
    weight = jnp.zeros((EP, rows), f32)
    for k in range(route_ref.shape[0]):
        same = route_ref[k : k + 1, :] == expert
        named = jnp.where(same, 1.0, named)
        weight = jnp.where(same, weight_ref[k : k + 1, :], weight)
    before = lax.broadcasted_iota(jnp.int32, (rows, rows), 0) < lax.broadcasted_iota(
        jnp.int32, (rows, rows), 1
    )
    earlier = jnp.dot(named, before.astype(f32), preferred_element_type=f32)
    taken = per_slot(jnp.where(named > 0.0, earlier, -1.0))
    slot = (lax.broadcasted_iota(jnp.int32, taken.shape, 0) % CAP).astype(f32)
    here = taken == slot
    placing = jnp.where(here, 1.0, 0.0).astype(bf16)
    send_ref[...] = jnp.dot(placing, normed, preferred_element_type=f32).astype(bf16)
    chosen_ref[...] = jnp.where(here, per_slot(weight), 0.0).T


def expert_kernel(rows_ref, gate_ref, up_far, down_far, out_ref, up_ref, down_ref, sems):
    parts, _, share = rows_ref.shape
    spans = [slice(p * share, (p + 1) * share) for p in range(parts)]
    fetches = [
        pltpu.make_async_copy(up_far.at[:, cols], up_ref.at[:, cols], sems.at[p])
        for p, cols in enumerate(spans)
    ] + [
        pltpu.make_async_copy(down_far.at[:, cols], down_ref.at[:, cols], sems.at[parts + p])
        for p, cols in enumerate(spans)
    ]
    for fetch in fetches:
        fetch.start()
    contract = (((1,), (1,)), ((), ()))
    gate = up = None
    for p, cols in enumerate(spans):
        g = lax.dot_general(gate_ref[:, cols], rows_ref[p], contract, preferred_element_type=f32)
        gate = g if gate is None else gate + g
    for p, cols in enumerate(spans):
        fetches[p].wait()
        u = lax.dot_general(up_ref[:, cols], rows_ref[p], contract, preferred_element_type=f32)
        up = u if up is None else up + u
    hidden = (gate / (1.0 + jnp.exp(-gate)) * up).T.astype(bf16)
    block = share // Y
    for p, cols in enumerate(spans):
        fetches[parts + p].wait()
        sums = jnp.dot(hidden, down_ref[:, cols], preferred_element_type=f32).astype(bf16)
        for i in range(Y):
            y, x = divmod(p * Y + i, X)
            out_ref[x, :, y * block : (y + 1) * block] = sums[:, i * block : (i + 1) * block]


def sum_x_kernel(in_ref, out_ref):
    total = summed(in_ref).T
    block = total.shape[0] // Y
    half = block // 2
    for y in range(Y):
        piece = total[y * block : (y + 1) * block]
        out_ref[y, :block] = piece[:, :LANES].astype(bf16)
        tail = piece[:, LANES:]
        out_ref[y, block:] = jnp.concatenate([tail[:half], tail[half:]], axis=1).astype(bf16)


def sum_y_kernel(in_ref, out_ref):
    total = summed(in_ref)
    block = out_ref.shape[1]
    rest = out_ref.shape[0] - LANES
    tail = jnp.concatenate([total[block:, :rest], total[block:, rest:]], axis=0)
    out_ref[:LANES] = total[:block].T.astype(bf16)
    out_ref[LANES:] = tail.T.astype(bf16)


def mix_kernel(got_ref, chosen_ref, out_ref):
    mixed = jnp.dot(
        chosen_ref[...],
        got_ref[...].astype(f32),
        preferred_element_type=f32,
        precision=lax.Precision.HIGHEST,
    )
    out_ref[...] = mixed.astype(bf16)


def on_device(tokens, norm_gain, route, route_weight, gate_weight, up_weight, down_weight):
    tok_rows, width = tokens.shape
    quarter = width // X
    share = width // TP
    spots = EP * CAP
    ep = ("z", "c")
    at = lax.axis_index("x").astype(jnp.int32).reshape(1)

    inputs = (tokens, norm_gain, route.T, route_weight.T)
    send, chosen = local(
        place_kernel,
        "place",
        [pl.BlockSpec(memory_space=pltpu.SMEM)] + [HBM] * 4,
        (pltpu.VMEM((spots, quarter), bf16), pltpu.VMEM((tok_rows, spots), f32)),
        scratch=[pltpu.VMEM(a.shape, a.dtype) for a in inputs]
        + [pltpu.SemaphoreType.DMA((len(inputs),))],
    )(at, *[far(a) for a in inputs])
    arrived = lax.all_to_all(send.reshape(EP, CAP, quarter), ep, 0, 0, tiled=True)
    rows = lax.all_gather(arrived.reshape(spots, quarter), "x", axis=0, tiled=False)
    part = local(
        expert_kernel,
        "expert",
        [VMEM, VMEM, HBM, HBM],
        pltpu.VMEM((X, spots, quarter), bf16),
        scratch=[
            pltpu.VMEM(up_weight.shape[1:], bf16),
            pltpu.VMEM(down_weight.shape[1:], bf16),
            pltpu.SemaphoreType.DMA((2 * X,)),
        ],
    )(near(rows), near(gate_weight[0]), far(up_weight[0]), far(down_weight[0]))
    part = lax.all_to_all(part, "x", 0, 0, tiled=True)
    packed = spots * share // LANES
    part = local(sum_x_kernel, "sum_x", [VMEM], pltpu.VMEM((Y, packed, LANES), bf16))(near(part))
    part = lax.all_to_all(part, "y", 0, 0, tiled=True)
    done = local(sum_y_kernel, "sum_y", [VMEM], pltpu.VMEM((spots, share), bf16))(near(part))
    back = lax.all_to_all(done.reshape(EP, CAP, share), ep, 0, 0, tiled=True)
    mixed = jax.ShapeDtypeStruct((tok_rows, share), bf16)
    return local(mix_kernel, "mix", [VMEM, VMEM], mixed)(
        near(back.reshape(spots, share)), near(chosen)
    )


def solution(mesh):
    fine = Mesh(mesh.devices.reshape(Z, C, Y, X), ("z", "c", "y", "x"))
    ep, tp = ("z", "c"), ("y", "x")
    placed = (
        P(ep, None),
        P(),
        P(ep, None),
        P(ep, None),
        P(ep, tp, None),
        P(ep, tp, None),
        P(ep, tp, None),
    )
    return jax.shard_map(
        on_device, mesh=fine, in_specs=placed, out_specs=P(ep, tp), check_vma=False
    )
```

time: 136 us -> 101 us (0.74)
  waiting for transfers between devices: 46.3 us -> 0 us
  blocking collectives: 55.6 us -> 93.9 us
  starting transfers between devices: 17 us -> 0 us
  local copies, waits for them, and re-layouts: 7.15 us -> 0.01 us
  Pallas kernels: 0 us -> 6.95 us
  matrix products: 5.09 us -> 0 us
  other arithmetic: 4.23 us -> 0 us
    all_to_all x2 -> x0, waiting for transfers between devices: 46.3 us -> none  [the longest x1 36.1 us: sent_and_summed(): tiles = lax.all_to_all(split_up(shard, dim, size), axis, 0, 0, tiled=True)]
    all_to_all x1 -> x4, blocking collectives: 55.6 us -> 80.5 us  [the longest x1 31.4 us: on_device(): lax.all_to_all(send.reshape(EP, CAP, quarter), ep, 0, 0, tiled=True)]
    all_to_all x2 -> x0, starting transfers between devices: 17 us -> none  [the longest x1 9.79 us: sent_and_summed(): tiles = lax.all_to_all(split_up(shard, dim, size), axis, 0, 0, tiled=True)]
    all_gather x0 -> x1, blocking collectives: none -> 13.4 us  [on_device(): lax.all_gather(arrived.reshape(spots, quarter), 'x', axis=0, tiled=False)]
    pallas_call x0 -> x5, Pallas kernels: none -> 6.95 us  [the longest x1 4.3 us: on_device(): local(expert_kernel, 'expert', [VMEM, VMEM, HBM, HBM], pltpu.VMEM((X, spo...]
    reshape x4 -> x0, local copies, waits for them, and re-layouts: 5.1 us -> none  [the longest x2 4.85 us: split_up(): shard.reshape(*lengths[:dim], size, lengths[dim] // size, *lengths[dim +...]
    dot_general x3 -> x0, matrix products: 5.09 us -> none  [the longest x1 3.89 us: on_device(): jnp.einsum('sjcf,jfd->sjcd', hidden, down_weight, preferred_element_type=...]
    reduce_sum x4 -> x0, other arithmetic: 2.9 us -> none  [the longest x1 1.06 us: on_device(): jnp.mean(values * values, axis=-1, keepdims=True) + epsilon]
  transfers between devices with their start and end apart: 2 -> 0, of which waited for: 2 -> 0; matrix products, arithmetic and copies ran while one was open for 0% -> 0% of each run, Pallas kernels for 0% -> 0%
where the time goes in v2:
time: 101 us
  blocking collectives  93.9 us (93%)
  Pallas kernels  6.95 us (7%)
    all_to_all x1, blocking collectives, on_device(): lax.all_to_all(send.reshape(EP, CAP, quarter), ep, 0, 0, tiled=True)  31.4 us
    all_to_all x1, blocking collectives, on_device(): back = lax.all_to_all(done.reshape(EP, CAP, share), ep, 0, 0, tiled=True)  21.3 us
    all_to_all x1, blocking collectives, on_device(): part = lax.all_to_all(part, 'y', 0, 0, tiled=True)  15.8 us
    all_gather x1, blocking collectives, on_device(): lax.all_gather(arrived.reshape(spots, quarter), 'x', axis=0, tiled=False)  13.4 us
    all_to_all x1, blocking collectives, on_device(): part = lax.all_to_all(part, 'x', 0, 0, tiled=True)  12.1 us
    pallas_call x1, Pallas kernels, on_device(): local(expert_kernel, 'expert', [VMEM, VMEM, HBM, HBM], pltpu.VMEM((X, spo...  4.3 us

profile of v2, /device:TPU:1, one launch (start us, length us, event | category | flops | bytes accessed | tf_op | source)
XLA Modules:
  0.0 100.9 jit_solution(11876398788364861567)
XLA Ops:
  0.0 0.0 copy-start
  0.0 1.4 %place.1 = (bf16[192,640]{1,0:T(8,128)(2,1)S(1)}, f32[32,192]{1,0:T(8,128)S(1)}) custom-call(s32[1]{0:T(128)} %bitcast.at_ref, bf16[32,2560]{1,0:T(8,128)(2,1)} %refs_0_.1, f32[2560]{0:T(1024)} %refs_1_.1, s32[4,32]{1,0:T(4,128)} %bitcast.17, f32[4,32]{1,0:T(4,128)} %bitcast.18), custom_call_target="tpu_custom_call" | custom-call | tf_op jit(solution)/shard_map/place/pallas_call | solution.py:166
  1.4 31.4 %all_to_all.20 = bf16[24,8,640]{2,1,0:T(8,128)(2,1)S(1)} all-to-all(bf16[24,8,640]{2,1,0:T(8,128)(2,1)S(1)} %bitcast.11), channel_id=1, replica_groups=mesh['z'=12,'c'=2,'y'=8,'x'=4] {'z','c'}, dimensions={0} | all-to-all | bytes 491520 | tf_op jit(solution)/shard_map/all_to_all | solution.py:174
  32.8 13.4 %all_gather.3.rows_ref = bf16[4,192,640]{2,1,0:T(8,128)(2,1)S(1)} all-gather(bf16[1,192,640]{2,1,0:T(8,128)(2,1)S(1)} %bitcast.16), channel_id=1, replica_groups=mesh['z'=12,'c'=2,'y'=8,'x'=4] {'x'}, dimensions={0}, use_global_device_ids=true | all-gather | bytes 1228800 | tf_op jit(solution)/shard_map/all_gather | solution.py:175
  46.2 0.0 copy-done
  46.2 4.3 %expert.1 = bf16[4,192,640]{2,1,0:T(8,128)(2,1)S(1)} custom-call(bf16[4,192,640]{2,1,0:T(8,128)(2,1)S(1)} %all_gather.3.rows_ref, bf16[280,2560]{1,0:T(8,128)(2,1)S(1)} %bitcast.10, bf16[280,2560]{1,0:T(8,128)(2,1)} %bitcast.14, bf16[280,2560]{1,0:T(8,128)(2,1)} %bitcast.15), custom_call_target="tpu_custom_call" | custom-call | tf_op jit(solution)/shard_map/expert/pallas_call | solution.py:176
  50.5 12.1 %all_to_all.21.in_ref = bf16[4,192,640]{2,1,0:T(8,128)(2,1)S(1)} all-to-all(bf16[4,192,640]{2,1,0:T(8,128)(2,1)S(1)} %expert.1), channel_id=1, replica_groups=mesh['z'=12,'c'=2,'y'=8,'x'=4] {'x'}, dimensions={0} | all-to-all | bytes 1966080 | tf_op jit(solution)/shard_map/all_to_all | solution.py:187
  62.6 0.3 sum_x.1
  62.9 15.8 %all_to_all.22.in_ref = bf16[8,120,128]{2,1,0:T(8,128)(2,1)S(1)} all-to-all(bf16[8,120,128]{2,1,0:T(8,128)(2,1)S(1)} %sum_x.1), channel_id=1, replica_groups=mesh['z'=12,'c'=2,'y'=8,'x'=4] {'y'}, dimensions={0} | all-to-all | bytes 491520 | tf_op jit(solution)/shard_map/all_to_all | solution.py:190
  78.7 0.1 sum_y.1
  78.8 21.3 %all_to_all.23 = bf16[24,8,80]{2,1,0:T(8,128)(2,1)S(1)} all-to-all(bf16[24,8,80]{2,1,0:T(8,128)(2,1)S(1)} %bitcast.12), channel_id=1, replica_groups=mesh['z'=12,'c'=2,'y'=8,'x'=4] {'z','c'}, dimensions={0} | all-to-all | bytes 61440 | tf_op jit(solution)/shard_map/all_to_all | solution.py:192
  100.1 0.8 mix.1
Async XLA Ops:
  0.0 46.2 %copy-start = (bf16[1,280,2560]{2,1,0:T(8,128)(2,1)S(1)}, bf16[1,280,2560]{2,1,0:T(8,128)(2,1)}, u32[]{:S(2)}) copy-start(bf16[1,280,2560]{2,1,0:T(8,128)(2,1)} %param.11) | copy-start | bytes 4300804

commit v3 on v2

--- a/solution.py
+++ b/solution.py
@@ -30,13 +30,14 @@
     return pltpu.with_memory_space_constraint(array, pltpu.HBM)
 
 
-def local(kernel, name, specs, outs, scratch=()):
+def local(kernel, name, specs, outs, scratch=(), cost=None):
     return pl.pallas_call(
         kernel,
         in_specs=specs,
         out_specs=tuple(VMEM for _ in outs) if isinstance(outs, tuple) else VMEM,
         out_shape=outs,
         scratch_shapes=scratch,
+        cost_estimate=cost,
         compiler_params=pltpu.CompilerParams(vmem_limit_bytes=SCOPED),
         name=name,
     )
@@ -55,7 +56,7 @@
     return jnp.concatenate(lines, axis=0)
 
 
-def place_kernel(at_ref, *refs):
+def place_kernel(*refs):
     sources, (send_ref, chosen_ref) = refs[:4], refs[4:6]
     (tokens_ref, gain_ref, route_ref, weight_ref), sems = refs[6:10], refs[10]
     copies = [
@@ -70,7 +71,7 @@
     share = send_ref.shape[1]
     values = tokens_ref[...].astype(f32)
     scale = lax.rsqrt(jnp.mean(values * values, axis=-1, keepdims=True) + epsilon)
-    start = pl.multiple_of(at_ref[0] * share, LANES)
+    start = pl.multiple_of(lax.axis_index("x") * share, LANES)
     own = tokens_ref[:, pl.ds(start, share)].astype(f32)
     gain = gain_ref[pl.ds(start, share)].reshape(1, share)
     normed = (own * scale * gain).astype(bf16)
@@ -93,31 +94,20 @@
     chosen_ref[...] = jnp.where(here, per_slot(weight), 0.0).T
 
 
-def expert_kernel(rows_ref, gate_ref, up_far, down_far, out_ref, up_ref, down_ref, sems):
+def expert_kernel(rows_ref, gate_ref, up_ref, down_ref, out_ref):
     parts, _, share = rows_ref.shape
     spans = [slice(p * share, (p + 1) * share) for p in range(parts)]
-    fetches = [
-        pltpu.make_async_copy(up_far.at[:, cols], up_ref.at[:, cols], sems.at[p])
-        for p, cols in enumerate(spans)
-    ] + [
-        pltpu.make_async_copy(down_far.at[:, cols], down_ref.at[:, cols], sems.at[parts + p])
-        for p, cols in enumerate(spans)
-    ]
-    for fetch in fetches:
-        fetch.start()
     contract = (((1,), (1,)), ((), ()))
     gate = up = None
     for p, cols in enumerate(spans):
         g = lax.dot_general(gate_ref[:, cols], rows_ref[p], contract, preferred_element_type=f32)
         gate = g if gate is None else gate + g
     for p, cols in enumerate(spans):
-        fetches[p].wait()
         u = lax.dot_general(up_ref[:, cols], rows_ref[p], contract, preferred_element_type=f32)
         up = u if up is None else up + u
     hidden = (gate / (1.0 + jnp.exp(-gate)) * up).T.astype(bf16)
     block = share // Y
     for p, cols in enumerate(spans):
-        fetches[parts + p].wait()
         sums = jnp.dot(hidden, down_ref[:, cols], preferred_element_type=f32).astype(bf16)
         for i in range(Y):
             y, x = divmod(p * Y + i, X)
@@ -160,30 +150,24 @@
     share = width // TP
     spots = EP * CAP
     ep = ("z", "c")
-    at = lax.axis_index("x").astype(jnp.int32).reshape(1)
-
     inputs = (tokens, norm_gain, route.T, route_weight.T)
     send, chosen = local(
         place_kernel,
         "place",
-        [pl.BlockSpec(memory_space=pltpu.SMEM)] + [HBM] * 4,
+        [HBM] * 4,
         (pltpu.VMEM((spots, quarter), bf16), pltpu.VMEM((tok_rows, spots), f32)),
         scratch=[pltpu.VMEM(a.shape, a.dtype) for a in inputs]
         + [pltpu.SemaphoreType.DMA((len(inputs),))],
-    )(at, *[far(a) for a in inputs])
+        cost=pl.CostEstimate(flops=10**10, transcendentals=0, bytes_accessed=10**6),
+    )(*[far(a) for a in inputs])
     arrived = lax.all_to_all(send.reshape(EP, CAP, quarter), ep, 0, 0, tiled=True)
     rows = lax.all_gather(arrived.reshape(spots, quarter), "x", axis=0, tiled=False)
     part = local(
         expert_kernel,
         "expert",
-        [VMEM, VMEM, HBM, HBM],
+        [VMEM] * 4,
         pltpu.VMEM((X, spots, quarter), bf16),
-        scratch=[
-            pltpu.VMEM(up_weight.shape[1:], bf16),
-            pltpu.VMEM(down_weight.shape[1:], bf16),
-            pltpu.SemaphoreType.DMA((2 * X,)),
-        ],
-    )(near(rows), near(gate_weight[0]), far(up_weight[0]), far(down_weight[0]))
+    )(near(rows), near(gate_weight[0]), near(up_weight[0]), near(down_weight[0]))
     part = lax.all_to_all(part, "x", 0, 0, tiled=True)
     packed = spots * share // LANES
     part = local(sum_x_kernel, "sum_x", [VMEM], pltpu.VMEM((Y, packed, LANES), bf16))(near(part))

time: 101 us -> 99.2 us (0.982)
  Pallas kernels: 6.95 us -> 4.83 us
    pallas_call x2, Pallas kernels: 5.7 us -> 3.58 us  [the longest x1 2.14 us: on_device(): local(expert_kernel, 'expert', [VMEM] * 4, pltpu.VMEM((X, spots, quarter)...]
where the time goes in v3:
time: 99.2 us; the launch traced here: 98.9 us
  blocking collectives  94 us (95%)
  Pallas kernels  4.83 us (5%)
    all_to_all x1, blocking collectives, on_device(): lax.all_to_all(send.reshape(EP, CAP, quarter), ep, 0, 0, tiled=True)  31.5 us
    all_to_all x1, blocking collectives, on_device(): back = lax.all_to_all(done.reshape(EP, CAP, share), ep, 0, 0, tiled=True)  21.2 us
    all_to_all x1, blocking collectives, on_device(): part = lax.all_to_all(part, 'y', 0, 0, tiled=True)  15.8 us
    all_gather x1, blocking collectives, on_device(): lax.all_gather(arrived.reshape(spots, quarter), 'x', axis=0, tiled=False)  13.3 us
    all_to_all x1, blocking collectives, on_device(): part = lax.all_to_all(part, 'x', 0, 0, tiled=True)  12.1 us
    pallas_call x1, Pallas kernels, on_device(): local(expert_kernel, 'expert', [VMEM] * 4, pltpu.VMEM((X, spots, quarter)...  2.14 us

profile of v3, /device:TPU:1, one launch (start us, length us, event | category | flops | bytes accessed | tf_op | source)
XLA Modules:
  0.0 98.9 jit_solution(7920324133407060352)
XLA Ops:
  0.0 0.0 copy-start.1
  0.0 0.0 copy-start.2
  0.0 1.4 %place.1 = (bf16[192,640]{1,0:T(8,128)(2,1)S(1)}, f32[32,192]{1,0:T(8,128)S(1)}) custom-call(bf16[32,2560]{1,0:T(8,128)(2,1)} %refs_0_.1, f32[2560]{0:T(1024)} %refs_1_.1, s32[4,32]{1,0:T(4,128)} %bitcast.16, f32[4,32]{1,0:T(4,128)} %bitcast.17), custom_call_target="tpu_custom_call" | custom-call | flops 10000000000 | bytes 1000000 | tf_op jit(solution)/shard_map/place/pallas_call | solution.py:154
  1.5 0.0 copy-start
  1.5 31.5 %all_to_all.20 = bf16[24,8,640]{2,1,0:T(8,128)(2,1)S(1)} all-to-all(bf16[24,8,640]{2,1,0:T(8,128)(2,1)S(1)} %bitcast.12), channel_id=1, replica_groups=mesh['z'=12,'c'=2,'y'=8,'x'=4] {'z','c'}, dimensions={0} | all-to-all | bytes 491520 | tf_op jit(solution)/shard_map/all_to_all | solution.py:163
  33.0 13.3 %all_gather.3.rows_ref = bf16[4,192,640]{2,1,0:T(8,128)(2,1)S(1)} all-gather(bf16[1,192,640]{2,1,0:T(8,128)(2,1)S(1)} %bitcast.15), channel_id=1, replica_groups=mesh['z'=12,'c'=2,'y'=8,'x'=4] {'x'}, dimensions={0}, use_global_device_ids=true | all-gather | bytes 1228800 | tf_op jit(solution)/shard_map/all_gather | solution.py:164
  46.3 0.0 copy-done.1
  46.4 0.0 copy-done.2
  46.4 0.0 copy-done
  46.4 2.1 %expert.1 = bf16[4,192,640]{2,1,0:T(8,128)(2,1)S(1)} custom-call(bf16[4,192,640]{2,1,0:T(8,128)(2,1)S(1)} %all_gather.3.rows_ref, bf16[280,2560]{1,0:T(8,128)(2,1)S(1)} %bitcast.9, bf16[280,2560]{1,0:T(8,128)(2,1)S(1)} %bitcast.10, bf16[280,2560]{1,0:T(8,128)(2,1)S(1)} %bitcast.11), custom_call_target="tpu_custom_call" | custom-call | tf_op jit(solution)/shard_map/expert/pallas_call | solution.py:165
  48.5 12.1 %all_to_all.21.in_ref = bf16[4,192,640]{2,1,0:T(8,128)(2,1)S(1)} all-to-all(bf16[4,192,640]{2,1,0:T(8,128)(2,1)S(1)} %expert.1), channel_id=1, replica_groups=mesh['z'=12,'c'=2,'y'=8,'x'=4] {'x'}, dimensions={0} | all-to-all | bytes 1966080 | tf_op jit(solution)/shard_map/all_to_all | solution.py:171
  60.6 0.3 sum_x.1
  60.9 15.8 %all_to_all.22.in_ref = bf16[8,120,128]{2,1,0:T(8,128)(2,1)S(1)} all-to-all(bf16[8,120,128]{2,1,0:T(8,128)(2,1)S(1)} %sum_x.1), channel_id=1, replica_groups=mesh['z'=12,'c'=2,'y'=8,'x'=4] {'y'}, dimensions={0} | all-to-all | bytes 491520 | tf_op jit(solution)/shard_map/all_to_all | solution.py:174
  76.7 0.1 sum_y.1
  76.9 21.2 %all_to_all.23 = bf16[24,8,80]{2,1,0:T(8,128)(2,1)S(1)} all-to-all(bf16[24,8,80]{2,1,0:T(8,128)(2,1)S(1)} %bitcast.13), channel_id=1, replica_groups=mesh['z'=12,'c'=2,'y'=8,'x'=4] {'z','c'}, dimensions={0} | all-to-all | bytes 61440 | tf_op jit(solution)/shard_map/all_to_all | solution.py:176
  98.1 0.8 mix.1
Async XLA Ops:
  0.0 46.4 %copy-start.1 = (bf16[1,280,2560]{2,1,0:T(8,128)(2,1)S(1)}, bf16[1,280,2560]{2,1,0:T(8,128)(2,1)}, u32[]{:S(2)}) copy-start(bf16[1,280,2560]{2,1,0:T(8,128)(2,1)} %param.12) | copy-start | bytes 4300804
  0.0 46.4 %copy-start.2 = (bf16[1,280,2560]{2,1,0:T(8,128)(2,1)S(1)}, bf16[1,280,2560]{2,1,0:T(8,128)(2,1)}, u32[]{:S(2)}) copy-start(bf16[1,280,2560]{2,1,0:T(8,128)(2,1)} %param.13) | copy-start | bytes 4300804
  1.5 44.9 %copy-start = (bf16[1,280,2560]{2,1,0:T(8,128)(2,1)S(1)}, bf16[1,280,2560]{2,1,0:T(8,128)(2,1)}, u32[]{:S(2)}) copy-start(bf16[1,280,2560]{2,1,0:T(8,128)(2,1)} %param.11) | copy-start | bytes 4300804

commit v4 on v3

v4 whole, which is shorter than its diff:
```python
import jax
import jax.numpy as jnp
from jax import lax
from jax.experimental import pallas as pl
from jax.experimental.pallas import tpu as pltpu
from jax.sharding import Mesh
from jax.sharding import PartitionSpec as P

epsilon = 1e-06
bf16 = jnp.bfloat16
f32 = jnp.float32

Z, C, Y, X = 12, 2, 8, 4
EP = Z * C
TP = Y * X
CAP = 8
LANES = 128
SCOPED = 16 << 20
VMEM = pl.BlockSpec(memory_space=pltpu.VMEM)


HBM = pl.BlockSpec(memory_space=pl.ANY)


def near(array):
    return pltpu.with_memory_space_constraint(array, pltpu.VMEM)


def far(array):
    return pltpu.with_memory_space_constraint(array, pltpu.HBM)


def local(kernel, name, specs, outs, scratch=(), cost=None):
    return pl.pallas_call(
        kernel,
        in_specs=specs,
        out_specs=tuple(VMEM for _ in outs) if isinstance(outs, tuple) else VMEM,
        out_shape=outs,
        scratch_shapes=scratch,
        cost_estimate=cost,
        compiler_params=pltpu.CompilerParams(vmem_limit_bytes=SCOPED),
        name=name,
    )


def summed(ref):
    total = ref[0].astype(f32)
    for p in range(1, ref.shape[0]):
        total = total + ref[p].astype(f32)
    return total


def per_slot(table):
    rows = table.shape[1]
    lines = [jnp.broadcast_to(table[e : e + 1, :], (CAP, rows)) for e in range(table.shape[0])]
    return jnp.concatenate(lines, axis=0)


def place_kernel(*refs):
    sources, (send_ref, chosen_ref) = refs[:4], refs[4:6]
    (tokens_ref, gain_ref, route_ref, weight_ref), sems = refs[6:10], refs[10]
    copies = [
        pltpu.make_async_copy(source, there, sems.at[i])
        for i, (source, there) in enumerate(zip(sources, refs[6:10]))
    ]
    for i in (2, 3, 0, 1):
        copies[i].start()
    rows = tokens_ref.shape[0]
    share = send_ref.shape[1]
    before = lax.broadcasted_iota(jnp.int32, (rows, rows), 0) < lax.broadcasted_iota(
        jnp.int32, (rows, rows), 1
    )
    expert = lax.broadcasted_iota(jnp.int32, (EP, rows), 0)
    copies[2].wait()
    copies[3].wait()
    named = jnp.zeros((EP, rows), f32)
    weight = jnp.zeros((EP, rows), f32)
    for k in range(route_ref.shape[0]):
        same = route_ref[k : k + 1, :] == expert
        named = jnp.where(same, 1.0, named)
        weight = jnp.where(same, weight_ref[k : k + 1, :], weight)
    earlier = jnp.dot(named, before.astype(f32), preferred_element_type=f32)
    taken = per_slot(jnp.where(named > 0.0, earlier, -1.0))
    slot = (lax.broadcasted_iota(jnp.int32, taken.shape, 0) % CAP).astype(f32)
    here = taken == slot
    placing = jnp.where(here, 1.0, 0.0).astype(bf16)
    chosen_ref[...] = jnp.where(here, per_slot(weight), 0.0).T
    copies[0].wait()
    copies[1].wait()
    values = tokens_ref[...].astype(f32)
    scale = lax.rsqrt(jnp.mean(values * values, axis=-1, keepdims=True) + epsilon)
    start = pl.multiple_of(lax.axis_index("x") * share, LANES)
    own = tokens_ref[:, pl.ds(start, share)].astype(f32)
    gain = gain_ref[pl.ds(start, share)].reshape(1, share)
    normed = (own * scale * gain).astype(bf16)
    send_ref[...] = jnp.dot(placing, normed, preferred_element_type=f32).astype(bf16)


def expert_kernel(rows_ref, gate_ref, up_ref, down_ref, out_ref):
    parts, _, share = rows_ref.shape
    spans = [slice(p * share, (p + 1) * share) for p in range(parts)]
    contract = (((1,), (1,)), ((), ()))
    gate = up = None
    for p, cols in enumerate(spans):
        g = lax.dot_general(gate_ref[:, cols], rows_ref[p], contract, preferred_element_type=f32)
        gate = g if gate is None else gate + g
    for p, cols in enumerate(spans):
        u = lax.dot_general(up_ref[:, cols], rows_ref[p], contract, preferred_element_type=f32)
        up = u if up is None else up + u
    hidden = (gate / (1.0 + jnp.exp(-gate)) * up).astype(bf16).T
    block = share // Y
    for p, cols in enumerate(spans):
        sums = jnp.dot(hidden, down_ref[:, cols], preferred_element_type=f32).astype(bf16).T
        for i in range(Y):
            packed(sums[i * block : (i + 1) * block], out_ref.at[i], p)


def packed(piece, out, at):
    block = piece.shape[0]
    tail = piece[:, LANES:]
    out[at, :block] = piece[:, :LANES].astype(bf16)
    out[at, block:] = jnp.concatenate([tail[: block // 2], tail[block // 2 :]], axis=1).astype(bf16)


def sum_x_kernel(in_ref, out_ref):
    for q in range(in_ref.shape[1]):
        total = in_ref[0, q].astype(f32)
        for p in range(1, in_ref.shape[0]):
            total = total + in_ref[p, q].astype(f32)
        block = out_ref.shape[3]
        rest = EP * CAP - LANES
        tail = jnp.concatenate([total[block:, :rest], total[block:, rest:]], axis=0)
        out_ref[: LANES // CAP, q] = total[:block].T.reshape(LANES // CAP, CAP, block).astype(bf16)
        out_ref[LANES // CAP :, q] = tail.T.reshape(rest // CAP, CAP, block).astype(bf16)

def mix_kernel(got_ref, chosen_ref, out_ref):
    total = got_ref[:, 0].astype(f32)
    for q in range(1, got_ref.shape[1]):
        total = total + got_ref[:, q].astype(f32)
    mixed = jnp.dot(
        chosen_ref[...],
        total.reshape(EP * CAP, out_ref.shape[1]).astype(bf16).astype(f32),
        preferred_element_type=f32,
        precision=lax.Precision.HIGHEST,
    )
    out_ref[...] = mixed.astype(bf16)


def on_device(tokens, norm_gain, route, route_weight, gate_weight, up_weight, down_weight):
    tok_rows, width = tokens.shape
    quarter = width // X
    share = width // TP
    spots = EP * CAP
    ep = ("z", "c")
    inputs = (tokens, norm_gain, route.T, route_weight.T)
    send, chosen = local(
        place_kernel,
        "place",
        [HBM] * 4,
        (pltpu.VMEM((spots, quarter), bf16), pltpu.VMEM((tok_rows, spots), f32)),
        scratch=[pltpu.VMEM(a.shape, a.dtype) for a in inputs]
        + [pltpu.SemaphoreType.DMA((len(inputs),))],
        cost=pl.CostEstimate(flops=10**10, transcendentals=0, bytes_accessed=10**6),
    )(*[far(a) for a in inputs])
    arrived = lax.all_to_all(send.reshape(EP, CAP, quarter), ep, 0, 0, tiled=True)
    rows = lax.all_gather(arrived.reshape(spots, quarter), "x", axis=0, tiled=False)
    count = spots * share // LANES
    quads = Y // 2
    part = local(
        expert_kernel, "expert", [VMEM] * 4, pltpu.VMEM((2 * X, quads, count, LANES), bf16)
    )(near(rows), near(gate_weight[0]), near(up_weight[0]), near(down_weight[0]))
    part = lax.all_to_all(part, ("yp", "x"), 0, 0, tiled=True)
    part = local(sum_x_kernel, "sum_x", [VMEM], pltpu.VMEM((EP, quads, CAP, share), bf16))(
        near(part)
    )
    part = part.reshape(EP * quads, CAP, share)
    part = lax.all_to_all(part, ("z", "c", "yq"), 0, 0, tiled=True)
    back = part.reshape(EP, quads, CAP, share)
    mixed = jax.ShapeDtypeStruct((tok_rows, share), bf16)
    return local(mix_kernel, "mix", [VMEM, VMEM], mixed)(near(back), near(chosen))


def solution(mesh):
    fine = Mesh(mesh.devices.reshape(Z, C, Y // 2, 2, X), ("z", "c", "yq", "yp", "x"))
    ep, tp = ("z", "c"), ("yq", "yp", "x")
    placed = (
        P(ep, None),
        P(),
        P(ep, None),
        P(ep, None),
        P(ep, tp, None),
        P(ep, tp, None),
        P(ep, tp, None),
    )
    return jax.shard_map(
        on_device, mesh=fine, in_specs=placed, out_specs=P(ep, tp), check_vma=False
    )
```

time: 99.2 us -> 96.5 us (0.973)
  blocking collectives: 94 us -> 91.4 us
    all_to_all x3 -> x2, blocking collectives: 49.1 us -> 46.5 us  [the longest x1 33.2 us: on_device(): part = lax.all_to_all(part, ('z', 'c', 'yq'), 0, 0, tiled=True)]
    pallas_call x4 -> x3, Pallas kernels: 3.39 us -> 3.36 us  [the longest x1 2.29 us: on_device(): local(expert_kernel, 'expert', [VMEM] * 4, pltpu.VMEM((2 * X, quads, coun...]
where the time goes in v4:
time: 96.5 us; the launch traced here: 96.3 us
  blocking collectives  91.4 us (95%)
  Pallas kernels  4.82 us (5%)
    all_to_all x1, blocking collectives, on_device(): part = lax.all_to_all(part, ('z', 'c', 'yq'), 0, 0, tiled=True)  33.2 us
    all_to_all x1, blocking collectives, on_device(): lax.all_to_all(send.reshape(EP, CAP, quarter), ep, 0, 0, tiled=True)  31.5 us
    all_to_all x1, blocking collectives, on_device(): part = lax.all_to_all(part, ('yp', 'x'), 0, 0, tiled=True)  13.4 us
    all_gather x1, blocking collectives, on_device(): lax.all_gather(arrived.reshape(spots, quarter), 'x', axis=0, tiled=False)  13.3 us
    pallas_call x1, Pallas kernels, on_device(): local(expert_kernel, 'expert', [VMEM] * 4, pltpu.VMEM((2 * X, quads, coun...  2.29 us

profile of v4, /device:TPU:1, one launch (start us, length us, event | category | flops | bytes accessed | tf_op | source)
XLA Modules:
  0.0 96.3 jit_solution(14994493480270690286)
XLA Ops:
  0.0 0.0 copy-start.1
  0.0 0.0 copy-start.2
  0.0 1.5 %place.1 = (bf16[192,640]{1,0:T(8,128)(2,1)S(1)}, f32[32,192]{1,0:T(8,128)S(1)}) custom-call(bf16[32,2560]{1,0:T(8,128)(2,1)} %refs_0_.1, f32[2560]{0:T(1024)} %refs_1_.1, s32[4,32]{1,0:T(4,128)} %bitcast.16, f32[4,32]{1,0:T(4,128)} %bitcast.17), custom_call_target="tpu_custom_call" | custom-call | flops 10000000000 | bytes 1000000 | tf_op jit(solution)/shard_map/place/pallas_call | solution.py:156
  1.5 0.0 copy-start
  1.5 31.5 %all_to_all.15 = bf16[24,8,640]{2,1,0:T(8,128)(2,1)S(1)} all-to-all(bf16[24,8,640]{2,1,0:T(8,128)(2,1)S(1)} %bitcast.14), channel_id=1, replica_groups=mesh['z'=12,'c'=2,'yq'=4,'yp'=2,'x'=4] {'z','c'}, dimensions={0} | all-to-all | bytes 491520 | tf_op jit(solution)/shard_map/all_to_all | solution.py:165
  33.0 13.3 %all_gather.3.rows_ref = bf16[4,192,640]{2,1,0:T(8,128)(2,1)S(1)} all-gather(bf16[1,192,640]{2,1,0:T(8,128)(2,1)S(1)} %bitcast.15), channel_id=1, replica_groups=mesh['z'=12,'c'=2,'yq'=4,'yp'=2,'x'=4] {'x'}, dimensions={0}, use_global_device_ids=true | all-gather | bytes 1228800 | tf_op jit(solution)/shard_map/all_gather | solution.py:166
  46.3 0.0 copy-done.1
  46.3 0.0 copy-done.2
  46.3 0.0 copy-done
  46.4 2.3 %expert.1 = bf16[8,4,120,128]{3,2,1,0:T(8,128)(2,1)S(1)} custom-call(bf16[4,192,640]{2,1,0:T(8,128)(2,1)S(1)} %all_gather.3.rows_ref, bf16[280,2560]{1,0:T(8,128)(2,1)S(1)} %bitcast.9, bf16[280,2560]{1,0:T(8,128)(2,1)S(1)} %bitcast.10, bf16[280,2560]{1,0:T(8,128)(2,1)S(1)} %bitcast.11), custom_call_target="tpu_custom_call" | custom-call | tf_op jit(solution)/shard_map/expert/pallas_call | solution.py:169
  48.6 13.4 %all_to_all.16.in_ref = bf16[8,4,120,128]{3,2,1,0:T(8,128)(2,1)S(1)} all-to-all(bf16[8,4,120,128]{3,2,1,0:T(8,128)(2,1)S(1)} %expert.1), channel_id=1, replica_groups=mesh['z'=12,'c'=2,'yq'=4,'yp'=2,'x'=4] {'yp','x'}, dimensions={0} | all-to-all | bytes 1966080 | tf_op jit(solution)/shard_map/all_to_all | solution.py:172
  62.0 0.3 sum_x.1
  62.3 33.2 %all_to_all.17 = bf16[96,8,80]{2,1,0:T(8,128)(2,1)S(1)} all-to-all(bf16[96,8,80]{2,1,0:T(8,128)(2,1)S(1)} %bitcast.12), channel_id=1, replica_groups=mesh['z'=12,'c'=2,'yq'=4,'yp'=2,'x'=4] {'z','c','yq'}, dimensions={0} | all-to-all | bytes 245760 | tf_op jit(solution)/shard_map/all_to_all | solution.py:177
  95.5 0.8 mix.1
Async XLA Ops:
  0.0 46.3 %copy-start.1 = (bf16[1,280,2560]{2,1,0:T(8,128)(2,1)S(1)}, bf16[1,280,2560]{2,1,0:T(8,128)(2,1)}, u32[]{:S(2)}) copy-start(bf16[1,280,2560]{2,1,0:T(8,128)(2,1)} %param.12) | copy-start | bytes 4300804
  0.0 46.3 %copy-start.2 = (bf16[1,280,2560]{2,1,0:T(8,128)(2,1)S(1)}, bf16[1,280,2560]{2,1,0:T(8,128)(2,1)}, u32[]{:S(2)}) copy-start(bf16[1,280,2560]{2,1,0:T(8,128)(2,1)} %param.13) | copy-start | bytes 4300804
  1.5 44.9 %copy-start = (bf16[1,280,2560]{2,1,0:T(8,128)(2,1)S(1)}, bf16[1,280,2560]{2,1,0:T(8,128)(2,1)}, u32[]{:S(2)}) copy-start(bf16[1,280,2560]{2,1,0:T(8,128)(2,1)} %param.11) | copy-start | bytes 4300804

commit v5 on v4

--- a/solution.py
+++ b/solution.py
@@ -50,9 +50,9 @@
     return total
 
 
-def per_slot(table):
+def per_slot(table, order):
     rows = table.shape[1]
-    lines = [jnp.broadcast_to(table[e : e + 1, :], (CAP, rows)) for e in range(table.shape[0])]
+    lines = [jnp.broadcast_to(table[e : e + 1, :], (CAP, rows)) for e in order]
     return jnp.concatenate(lines, axis=0)
 
 
@@ -80,11 +80,12 @@
         named = jnp.where(same, 1.0, named)
         weight = jnp.where(same, weight_ref[k : k + 1, :], weight)
     earlier = jnp.dot(named, before.astype(f32), preferred_element_type=f32)
-    taken = per_slot(jnp.where(named > 0.0, earlier, -1.0))
-    slot = (lax.broadcasted_iota(jnp.int32, taken.shape, 0) % CAP).astype(f32)
-    here = taken == slot
-    placing = jnp.where(here, 1.0, 0.0).astype(bf16)
-    chosen_ref[...] = jnp.where(here, per_slot(weight), 0.0).T
+    spot = jnp.where(named > 0.0, earlier, -1.0)
+    slot = (lax.broadcasted_iota(jnp.int32, (EP * CAP, rows), 0) % CAP).astype(f32)
+    by_core = [z * C + c for c in range(C) for z in range(Z)]
+    placing = jnp.where(per_slot(spot, by_core) == slot, 1.0, 0.0).astype(bf16)
+    here = per_slot(spot, range(EP)) == slot
+    chosen_ref[...] = jnp.where(here, per_slot(weight, range(EP)), 0.0).T
     copies[0].wait()
     copies[1].wait()
     values = tokens_ref[...].astype(f32)
@@ -111,27 +112,30 @@
     block = share // Y
     for p, cols in enumerate(spans):
         sums = jnp.dot(hidden, down_ref[:, cols], preferred_element_type=f32).astype(bf16).T
-        for i in range(Y):
-            packed(sums[i * block : (i + 1) * block], out_ref.at[i], p)
-
-
-def packed(piece, out, at):
-    block = piece.shape[0]
-    tail = piece[:, LANES:]
-    out[at, :block] = piece[:, :LANES].astype(bf16)
-    out[at, block:] = jnp.concatenate([tail[: block // 2], tail[block // 2 :]], axis=1).astype(bf16)
+        half = sums.shape[1] // C
+        rest = LANES - half
+        for c in range(C):
+            for i in range(Y):
+                piece = sums[i * block : (i + 1) * block, c * half : (c + 1) * half]
+                if p < parts - 1:
+                    out_ref[c * Y + i, p, :, :half] = piece
+                    continue
+                for j in range(parts - 1):
+                    out_ref[c * Y + i, j, :, half:] = piece[:, j * rest : (j + 1) * rest]
 
 
 def sum_x_kernel(in_ref, out_ref):
-    for q in range(in_ref.shape[1]):
-        total = in_ref[0, q].astype(f32)
-        for p in range(1, in_ref.shape[0]):
-            total = total + in_ref[p, q].astype(f32)
-        block = out_ref.shape[3]
-        rest = EP * CAP - LANES
-        tail = jnp.concatenate([total[block:, :rest], total[block:, rest:]], axis=0)
-        out_ref[: LANES // CAP, q] = total[:block].T.reshape(LANES // CAP, CAP, block).astype(bf16)
-        out_ref[LANES // CAP :, q] = tail.T.reshape(rest // CAP, CAP, block).astype(bf16)
+    near_by, lines, block, _ = in_ref.shape
+    slots = out_ref.shape[0] * CAP
+    for c in range(C):
+        total = in_ref[c * Y].astype(f32)
+        for i in range(1, near_by // C):
+            total = total + in_ref[c * Y + i].astype(f32)
+        blocks = [total[q, :, :slots] for q in range(lines)]
+        blocks.append(jnp.concatenate([total[q, :, slots:] for q in range(lines)], axis=1))
+        for q, piece in enumerate(blocks):
+            out_ref[:, q, c] = piece.T.reshape(slots // CAP, CAP, block).astype(bf16)
+
 
 def mix_kernel(got_ref, chosen_ref, out_ref):
     total = got_ref[:, 0].astype(f32)
@@ -151,7 +155,6 @@
     quarter = width // X
     share = width // TP
     spots = EP * CAP
-    ep = ("z", "c")
     inputs = (tokens, norm_gain, route.T, route_weight.T)
     send, chosen = local(
         place_kernel,
@@ -162,20 +165,19 @@
         + [pltpu.SemaphoreType.DMA((len(inputs),))],
         cost=pl.CostEstimate(flops=10**10, transcendentals=0, bytes_accessed=10**6),
     )(*[far(a) for a in inputs])
-    arrived = lax.all_to_all(send.reshape(EP, CAP, quarter), ep, 0, 0, tiled=True)
+    arrived = lax.all_to_all(send.reshape(EP, CAP, quarter), ("c", "z"), 0, 0, tiled=True)
     rows = lax.all_gather(arrived.reshape(spots, quarter), "x", axis=0, tiled=False)
-    count = spots * share // LANES
     quads = Y // 2
     part = local(
-        expert_kernel, "expert", [VMEM] * 4, pltpu.VMEM((2 * X, quads, count, LANES), bf16)
+        expert_kernel, "expert", [VMEM] * 4, pltpu.VMEM((C * Y, quads - 1, share, LANES), bf16)
     )(near(rows), near(gate_weight[0]), near(up_weight[0]), near(down_weight[0]))
-    part = lax.all_to_all(part, ("yp", "x"), 0, 0, tiled=True)
-    part = local(sum_x_kernel, "sum_x", [VMEM], pltpu.VMEM((EP, quads, CAP, share), bf16))(
+    part = lax.all_to_all(part, ("c", "yp", "x"), 0, 0, tiled=True)
+    part = local(sum_x_kernel, "sum_x", [VMEM], pltpu.VMEM((Z, quads, C, CAP, share), bf16))(
         near(part)
     )
-    part = part.reshape(EP * quads, CAP, share)
-    part = lax.all_to_all(part, ("z", "c", "yq"), 0, 0, tiled=True)
-    back = part.reshape(EP, quads, CAP, share)
+    part = part.reshape(Z * quads, C * CAP, share)
+    part = lax.all_to_all(part, ("z", "yq"), 0, 0, tiled=True)
+    back = part.reshape(Z, quads, C, CAP, share)
     mixed = jax.ShapeDtypeStruct((tok_rows, share), bf16)
     return local(mix_kernel, "mix", [VMEM, VMEM], mixed)(near(back), near(chosen))
 

time: 96.5 us -> 98.6 us (1.022)
  blocking collectives: 91.4 us -> 92.9 us
    all_to_all x3, blocking collectives: 78.1 us -> 79.7 us  [the longest x1 31.9 us: on_device(): lax.all_to_all(send.reshape(EP, CAP, quarter), ('c', 'z'), 0, 0, tiled=True)]
where the time goes in v5:
time: 98.6 us; the launch traced here: 98.2 us
  blocking collectives  92.9 us (94%)
  Pallas kernels  5.26 us (5%)
    all_to_all x1, blocking collectives, on_device(): lax.all_to_all(send.reshape(EP, CAP, quarter), ('c', 'z'), 0, 0, tiled=True)  31.9 us
    all_to_all x1, blocking collectives, on_device(): part = lax.all_to_all(part, ('z', 'yq'), 0, 0, tiled=True)  25.4 us
    all_to_all x1, blocking collectives, on_device(): part = lax.all_to_all(part, ('c', 'yp', 'x'), 0, 0, tiled=True)  22.5 us
    all_gather x1, blocking collectives, on_device(): lax.all_gather(arrived.reshape(spots, quarter), 'x', axis=0, tiled=False)  13.2 us
    pallas_call x1, Pallas kernels, on_device(): local(expert_kernel, 'expert', [VMEM] * 4, pltpu.VMEM((C * Y, quads - 1,...  2.73 us

profile of v5, /device:TPU:1, one launch (start us, length us, event | category | flops | bytes accessed | tf_op | source)
XLA Modules:
  0.0 98.2 jit_solution(12510656362301998521)
XLA Ops:
  0.0 0.0 copy-start.1
  0.0 0.0 copy-start.2
  0.0 1.5 %place.1 = (bf16[192,640]{1,0:T(8,128)(2,1)S(1)}, f32[32,192]{1,0:T(8,128)S(1)}) custom-call(bf16[32,2560]{1,0:T(8,128)(2,1)} %refs_0_.1, f32[2560]{0:T(1024)} %refs_1_.1, s32[4,32]{1,0:T(4,128)} %bitcast.16, f32[4,32]{1,0:T(4,128)} %bitcast.17), custom_call_target="tpu_custom_call" | custom-call | flops 10000000000 | bytes 1000000 | tf_op jit(solution)/shard_map/place/pallas_call | solution.py:159
  1.5 0.0 copy-start
  1.5 31.9 %all_to_all.15 = bf16[24,8,640]{2,1,0:T(8,128)(2,1)S(1)} all-to-all(bf16[24,8,640]{2,1,0:T(8,128)(2,1)S(1)} %bitcast.14), channel_id=1, replica_groups=mesh['z'=12,'c'=2,'yq'=4,'yp'=2,'x'=4] {'c','z'}, dimensions={0} | all-to-all | bytes 491520 | tf_op jit(solution)/shard_map/all_to_all | solution.py:168
  33.4 13.2 %all_gather.3.rows_ref = bf16[4,192,640]{2,1,0:T(8,128)(2,1)S(1)} all-gather(bf16[1,192,640]{2,1,0:T(8,128)(2,1)S(1)} %bitcast.15), channel_id=1, replica_groups=mesh['z'=12,'c'=2,'yq'=4,'yp'=2,'x'=4] {'x'}, dimensions={0}, use_global_device_ids=true | all-gather | bytes 1228800 | tf_op jit(solution)/shard_map/all_gather | solution.py:169
  46.6 0.0 copy-done.1
  46.6 0.0 copy-done.2
  46.6 0.0 copy-done
  46.6 2.7 %expert.1 = bf16[16,3,80,128]{3,2,1,0:T(8,128)(2,1)S(1)} custom-call(bf16[4,192,640]{2,1,0:T(8,128)(2,1)S(1)} %all_gather.3.rows_ref, bf16[280,2560]{1,0:T(8,128)(2,1)S(1)} %bitcast.9, bf16[280,2560]{1,0:T(8,128)(2,1)S(1)} %bitcast.10, bf16[280,2560]{1,0:T(8,128)(2,1)S(1)} %bitcast.11), custom_call_target="tpu_custom_call" | custom-call | tf_op jit(solution)/shard_map/expert/pallas_call | solution.py:171
  49.3 22.5 %all_to_all.16.in_ref = bf16[16,3,80,128]{3,2,1,0:T(8,128)(2,1)S(1)} all-to-all(bf16[16,3,80,128]{3,2,1,0:T(8,128)(2,1)S(1)} %expert.1), channel_id=1, replica_groups=mesh['z'=12,'c'=2,'yq'=4,'yp'=2,'x'=4] {'c','yp','x'}, dimensions={0} | all-to-all | bytes 1966080 | tf_op jit(solution)/shard_map/all_to_all | solution.py:174
  71.8 0.3 sum_x.1
  72.1 25.4 %all_to_all.17 = bf16[48,16,80]{2,1,0:T(8,128)(2,1)S(1)} all-to-all(bf16[48,16,80]{2,1,0:T(8,128)(2,1)S(1)} %bitcast.12), channel_id=1, replica_groups=mesh['z'=12,'c'=2,'yq'=4,'yp'=2,'x'=4] {'z','yq'}, dimensions={0} | all-to-all | bytes 245760 | tf_op jit(solution)/shard_map/all_to_all | solution.py:179
  97.4 0.8 mix.1
Async XLA Ops:
  0.0 46.6 %copy-start.1 = (bf16[1,280,2560]{2,1,0:T(8,128)(2,1)S(1)}, bf16[1,280,2560]{2,1,0:T(8,128)(2,1)}, u32[]{:S(2)}) copy-start(bf16[1,280,2560]{2,1,0:T(8,128)(2,1)} %param.12) | copy-start | bytes 4300804
  0.0 46.6 %copy-start.2 = (bf16[1,280,2560]{2,1,0:T(8,128)(2,1)S(1)}, bf16[1,280,2560]{2,1,0:T(8,128)(2,1)}, u32[]{:S(2)}) copy-start(bf16[1,280,2560]{2,1,0:T(8,128)(2,1)} %param.13) | copy-start | bytes 4300804
  1.5 45.1 %copy-start = (bf16[1,280,2560]{2,1,0:T(8,128)(2,1)S(1)}, bf16[1,280,2560]{2,1,0:T(8,128)(2,1)}, u32[]{:S(2)}) copy-start(bf16[1,280,2560]{2,1,0:T(8,128)(2,1)} %param.11) | copy-start | bytes 4300804

commit v6 on v4

--- a/solution.py
+++ b/solution.py
@@ -79,12 +79,18 @@
         same = route_ref[k : k + 1, :] == expert
         named = jnp.where(same, 1.0, named)
         weight = jnp.where(same, weight_ref[k : k + 1, :], weight)
-    earlier = jnp.dot(named, before.astype(f32), preferred_element_type=f32)
+    earlier = jnp.dot(
+        named.astype(bf16), before.astype(f32).astype(bf16), preferred_element_type=f32
+    )
     taken = per_slot(jnp.where(named > 0.0, earlier, -1.0))
     slot = (lax.broadcasted_iota(jnp.int32, taken.shape, 0) % CAP).astype(f32)
     here = taken == slot
     placing = jnp.where(here, 1.0, 0.0).astype(bf16)
-    chosen_ref[...] = jnp.where(here, per_slot(weight), 0.0).T
+    left = jnp.where(here, per_slot(weight), 0.0).T
+    for i in range(chosen_ref.shape[0]):
+        part = left.astype(bf16)
+        chosen_ref[i] = part
+        left = left - part.astype(f32)
     copies[0].wait()
     copies[1].wait()
     values = tokens_ref[...].astype(f32)
@@ -127,22 +133,22 @@
         total = in_ref[0, q].astype(f32)
         for p in range(1, in_ref.shape[0]):
             total = total + in_ref[p, q].astype(f32)
+        total = total.astype(bf16)
         block = out_ref.shape[3]
         rest = EP * CAP - LANES
         tail = jnp.concatenate([total[block:, :rest], total[block:, rest:]], axis=0)
-        out_ref[: LANES // CAP, q] = total[:block].T.reshape(LANES // CAP, CAP, block).astype(bf16)
-        out_ref[LANES // CAP :, q] = tail.T.reshape(rest // CAP, CAP, block).astype(bf16)
+        out_ref[: LANES // CAP, q] = total[:block].T.reshape(LANES // CAP, CAP, block)
+        out_ref[LANES // CAP :, q] = tail.T.reshape(rest // CAP, CAP, block)
+
 
 def mix_kernel(got_ref, chosen_ref, out_ref):
     total = got_ref[:, 0].astype(f32)
     for q in range(1, got_ref.shape[1]):
         total = total + got_ref[:, q].astype(f32)
-    mixed = jnp.dot(
-        chosen_ref[...],
-        total.reshape(EP * CAP, out_ref.shape[1]).astype(bf16).astype(f32),
-        preferred_element_type=f32,
-        precision=lax.Precision.HIGHEST,
-    )
+    rows = total.reshape(EP * CAP, out_ref.shape[1]).astype(bf16)
+    mixed = jnp.dot(chosen_ref[0], rows, preferred_element_type=f32)
+    for i in range(1, chosen_ref.shape[0]):
+        mixed = mixed + jnp.dot(chosen_ref[i], rows, preferred_element_type=f32)
     out_ref[...] = mixed.astype(bf16)
 
 
@@ -157,7 +163,7 @@
         place_kernel,
         "place",
         [HBM] * 4,
-        (pltpu.VMEM((spots, quarter), bf16), pltpu.VMEM((tok_rows, spots), f32)),
+        (pltpu.VMEM((spots, quarter), bf16), pltpu.VMEM((3, tok_rows, spots), bf16)),
         scratch=[pltpu.VMEM(a.shape, a.dtype) for a in inputs]
         + [pltpu.SemaphoreType.DMA((len(inputs),))],
         cost=pl.CostEstimate(flops=10**10, transcendentals=0, bytes_accessed=10**6),

time: 96.5 us -> 96.4 us (level)
  no operation moved by 1% of the time
where the time goes in v6:
time: 96.4 us; the launch traced here: 96.2 us
  blocking collectives  91.4 us (95%)
  Pallas kernels  4.73 us (5%)
    all_to_all x1, blocking collectives, on_device(): part = lax.all_to_all(part, ('z', 'c', 'yq'), 0, 0, tiled=True)  33.2 us
    all_to_all x1, blocking collectives, on_device(): lax.all_to_all(send.reshape(EP, CAP, quarter), ep, 0, 0, tiled=True)  31.5 us
    all_to_all x1, blocking collectives, on_device(): part = lax.all_to_all(part, ('yp', 'x'), 0, 0, tiled=True)  13.4 us
    all_gather x1, blocking collectives, on_device(): lax.all_gather(arrived.reshape(spots, quarter), 'x', axis=0, tiled=False)  13.3 us
    pallas_call x1, Pallas kernels, on_device(): local(expert_kernel, 'expert', [VMEM] * 4, pltpu.VMEM((2 * X, quads, coun...  2.29 us

profile of v6, /device:TPU:1, one launch (start us, length us, event | category | flops | bytes accessed | tf_op | source)
XLA Modules:
  0.0 96.2 jit_solution(1908503146890081713)
XLA Ops:
  0.0 0.0 copy-start.1
  0.0 0.0 copy-start.2
  0.0 1.5 %place.1 = (bf16[192,640]{1,0:T(8,128)(2,1)S(1)}, bf16[3,32,192]{2,1,0:T(8,128)(2,1)S(1)}) custom-call(bf16[32,2560]{1,0:T(8,128)(2,1)} %refs_0_.1, f32[2560]{0:T(1024)} %refs_1_.1, s32[4,32]{1,0:T(4,128)} %bitcast.16, f32[4,32]{1,0:T(4,128)} %bitcast.17), custom_call_target="tpu_custom_call" | custom-call | flops 10000000000 | bytes 1000000 | tf_op jit(solution)/shard_map/place/pallas_call | solution.py:162
  1.5 0.0 copy-start
  1.5 31.5 %all_to_all.15 = bf16[24,8,640]{2,1,0:T(8,128)(2,1)S(1)} all-to-all(bf16[24,8,640]{2,1,0:T(8,128)(2,1)S(1)} %bitcast.14), channel_id=1, replica_groups=mesh['z'=12,'c'=2,'yq'=4,'yp'=2,'x'=4] {'z','c'}, dimensions={0} | all-to-all | bytes 491520 | tf_op jit(solution)/shard_map/all_to_all | solution.py:171
  33.0 13.3 %all_gather.3.rows_ref = bf16[4,192,640]{2,1,0:T(8,128)(2,1)S(1)} all-gather(bf16[1,192,640]{2,1,0:T(8,128)(2,1)S(1)} %bitcast.15), channel_id=1, replica_groups=mesh['z'=12,'c'=2,'yq'=4,'yp'=2,'x'=4] {'x'}, dimensions={0}, use_global_device_ids=true | all-gather | bytes 1228800 | tf_op jit(solution)/shard_map/all_gather | solution.py:172
  46.3 0.0 copy-done.1
  46.3 0.0 copy-done.2
  46.3 0.0 copy-done
  46.4 2.3 %expert.1 = bf16[8,4,120,128]{3,2,1,0:T(8,128)(2,1)S(1)} custom-call(bf16[4,192,640]{2,1,0:T(8,128)(2,1)S(1)} %all_gather.3.rows_ref, bf16[280,2560]{1,0:T(8,128)(2,1)S(1)} %bitcast.9, bf16[280,2560]{1,0:T(8,128)(2,1)S(1)} %bitcast.10, bf16[280,2560]{1,0:T(8,128)(2,1)S(1)} %bitcast.11), custom_call_target="tpu_custom_call" | custom-call | tf_op jit(solution)/shard_map/expert/pallas_call | solution.py:175
  48.6 13.4 %all_to_all.16.in_ref = bf16[8,4,120,128]{3,2,1,0:T(8,128)(2,1)S(1)} all-to-all(bf16[8,4,120,128]{3,2,1,0:T(8,128)(2,1)S(1)} %expert.1), channel_id=1, replica_groups=mesh['z'=12,'c'=2,'yq'=4,'yp'=2,'x'=4] {'yp','x'}, dimensions={0} | all-to-all | bytes 1966080 | tf_op jit(solution)/shard_map/all_to_all | solution.py:178
  62.0 0.2 sum_x.1
  62.2 33.2 %all_to_all.17 = bf16[96,8,80]{2,1,0:T(8,128)(2,1)S(1)} all-to-all(bf16[96,8,80]{2,1,0:T(8,128)(2,1)S(1)} %bitcast.12), channel_id=1, replica_groups=mesh['z'=12,'c'=2,'yq'=4,'yp'=2,'x'=4] {'z','c','yq'}, dimensions={0} | all-to-all | bytes 245760 | tf_op jit(solution)/shard_map/all_to_all | solution.py:183
  95.4 0.8 mix.1
Async XLA Ops:
  0.0 46.3 %copy-start.1 = (bf16[1,280,2560]{2,1,0:T(8,128)(2,1)S(1)}, bf16[1,280,2560]{2,1,0:T(8,128)(2,1)}, u32[]{:S(2)}) copy-start(bf16[1,280,2560]{2,1,0:T(8,128)(2,1)} %param.12) | copy-start | bytes 4300804
  0.0 46.3 %copy-start.2 = (bf16[1,280,2560]{2,1,0:T(8,128)(2,1)S(1)}, bf16[1,280,2560]{2,1,0:T(8,128)(2,1)}, u32[]{:S(2)}) copy-start(bf16[1,280,2560]{2,1,0:T(8,128)(2,1)} %param.13) | copy-start | bytes 4300804
  1.5 44.9 %copy-start = (bf16[1,280,2560]{2,1,0:T(8,128)(2,1)S(1)}, bf16[1,280,2560]{2,1,0:T(8,128)(2,1)}, u32[]{:S(2)}) copy-start(bf16[1,280,2560]{2,1,0:T(8,128)(2,1)} %param.11) | copy-start | bytes 4300804

commit v7 on v6

--- a/solution.py
+++ b/solution.py
@@ -56,41 +56,37 @@
     return jnp.concatenate(lines, axis=0)
 
 
+def spots_of(route_ref):
+    rows = route_ref.shape[1]
+    expert = lax.broadcasted_iota(jnp.int32, (EP, rows), 0)
+    same = [route_ref[k : k + 1, :] == expert for k in range(route_ref.shape[0])]
+    named = jnp.zeros((EP, rows), f32)
+    for hit in same:
+        named = jnp.where(hit, 1.0, named)
+    before = lax.broadcasted_iota(jnp.int32, (rows, rows), 0) < lax.broadcasted_iota(
+        jnp.int32, (rows, rows), 1
+    )
+    earlier = jnp.dot(
+        named.astype(bf16), before.astype(f32).astype(bf16), preferred_element_type=f32
+    )
+    taken = per_slot(jnp.where(named > 0.0, earlier, -1.0))
+    slot = (lax.broadcasted_iota(jnp.int32, taken.shape, 0) % CAP).astype(f32)
+    return same, taken == slot
+
+
 def place_kernel(*refs):
-    sources, (send_ref, chosen_ref) = refs[:4], refs[4:6]
-    (tokens_ref, gain_ref, route_ref, weight_ref), sems = refs[6:10], refs[10]
+    sources, send_ref = refs[:3], refs[3]
+    (tokens_ref, gain_ref, route_ref), sems = refs[4:7], refs[7]
     copies = [
         pltpu.make_async_copy(source, there, sems.at[i])
-        for i, (source, there) in enumerate(zip(sources, refs[6:10]))
+        for i, (source, there) in enumerate(zip(sources, refs[4:7]))
     ]
-    for i in (2, 3, 0, 1):
+    for i in (2, 0, 1):
         copies[i].start()
-    rows = tokens_ref.shape[0]
     share = send_ref.shape[1]
-    before = lax.broadcasted_iota(jnp.int32, (rows, rows), 0) < lax.broadcasted_iota(
-        jnp.int32, (rows, rows), 1
-    )
-    expert = lax.broadcasted_iota(jnp.int32, (EP, rows), 0)
     copies[2].wait()
-    copies[3].wait()
-    named = jnp.zeros((EP, rows), f32)
-    weight = jnp.zeros((EP, rows), f32)
-    for k in range(route_ref.shape[0]):
-        same = route_ref[k : k + 1, :] == expert
-        named = jnp.where(same, 1.0, named)
-        weight = jnp.where(same, weight_ref[k : k + 1, :], weight)
-    earlier = jnp.dot(
-        named.astype(bf16), before.astype(f32).astype(bf16), preferred_element_type=f32
-    )
-    taken = per_slot(jnp.where(named > 0.0, earlier, -1.0))
-    slot = (lax.broadcasted_iota(jnp.int32, taken.shape, 0) % CAP).astype(f32)
-    here = taken == slot
+    _, here = spots_of(route_ref)
     placing = jnp.where(here, 1.0, 0.0).astype(bf16)
-    left = jnp.where(here, per_slot(weight), 0.0).T
-    for i in range(chosen_ref.shape[0]):
-        part = left.astype(bf16)
-        chosen_ref[i] = part
-        left = left - part.astype(f32)
     copies[0].wait()
     copies[1].wait()
     values = tokens_ref[...].astype(f32)
@@ -100,6 +96,18 @@
     gain = gain_ref[pl.ds(start, share)].reshape(1, share)
     normed = (own * scale * gain).astype(bf16)
     send_ref[...] = jnp.dot(placing, normed, preferred_element_type=f32).astype(bf16)
+
+
+def weigh_kernel(route_ref, weight_ref, chosen_ref):
+    same, here = spots_of(route_ref)
+    weight = jnp.zeros((EP, route_ref.shape[1]), f32)
+    for k, hit in enumerate(same):
+        weight = jnp.where(hit, weight_ref[k : k + 1, :], weight)
+    left = jnp.where(here, per_slot(weight), 0.0).T
+    for i in range(chosen_ref.shape[0]):
+        part = left.astype(bf16)
+        chosen_ref[i] = part
+        left = left - part.astype(f32)
 
 
 def expert_kernel(rows_ref, gate_ref, up_ref, down_ref, out_ref):
@@ -158,16 +166,23 @@
     share = width // TP
     spots = EP * CAP
     ep = ("z", "c")
-    inputs = (tokens, norm_gain, route.T, route_weight.T)
-    send, chosen = local(
+    inputs = (tokens, norm_gain, route.T)
+    send = local(
         place_kernel,
         "place",
-        [HBM] * 4,
-        (pltpu.VMEM((spots, quarter), bf16), pltpu.VMEM((3, tok_rows, spots), bf16)),
+        [HBM] * 3,
+        pltpu.VMEM((spots, quarter), bf16),
         scratch=[pltpu.VMEM(a.shape, a.dtype) for a in inputs]
         + [pltpu.SemaphoreType.DMA((len(inputs),))],
         cost=pl.CostEstimate(flops=10**10, transcendentals=0, bytes_accessed=10**6),
     )(*[far(a) for a in inputs])
+    chosen = local(
+        weigh_kernel,
+        "weigh",
+        [VMEM] * 2,
+        pltpu.VMEM((3, tok_rows, spots), bf16),
+        cost=pl.CostEstimate(flops=10**9, transcendentals=0, bytes_accessed=10**5),
+    )(near(route.T), near(route_weight.T))
     arrived = lax.all_to_all(send.reshape(EP, CAP, quarter), ep, 0, 0, tiled=True)
     rows = lax.all_gather(arrived.reshape(spots, quarter), "x", axis=0, tiled=False)
     count = spots * share // LANES

time: 96.4 us -> 97.5 us (1.011)
  blocking collectives: 91.4 us -> 58.4 us
  waiting for transfers between devices: 0 us -> 17.5 us
  starting transfers between devices: 0 us -> 15.7 us
    all_to_all x1 -> x0, blocking collectives: 33.2 us -> none  [on_device(): part = lax.all_to_all(part, ('z', 'c', 'yq'), 0, 0, tiled=True)]
    all_to_all x0 -> x1, waiting for transfers between devices: none -> 17.5 us  [on_device(): part = lax.all_to_all(part, ('z', 'c', 'yq'), 0, 0, tiled=True)]
    all_to_all x0 -> x1, starting transfers between devices: none -> 15.7 us  [on_device(): part = lax.all_to_all(part, ('z', 'c', 'yq'), 0, 0, tiled=True)]
  transfers between devices with their start and end apart: 0 -> 1, of which waited for: 0 -> 1; matrix products, arithmetic and copies ran while one was open for 0% -> 0% of each run, Pallas kernels for 0% -> 0%
where the time goes in v7:
time: 97.5 us; the launch traced here: 97.2 us
  blocking collectives  58.4 us (60%)
  waiting for transfers between devices  17.5 us (18%)
  starting transfers between devices  15.7 us (16%)
  Pallas kernels  5.58 us (6%)
    all_to_all x1, blocking collectives, on_device(): lax.all_to_all(send.reshape(EP, CAP, quarter), ep, 0, 0, tiled=True)  31.5 us
    all_to_all x1, waiting for transfers between devices, on_device(): part = lax.all_to_all(part, ('z', 'c', 'yq'), 0, 0, tiled=True)  17.5 us
    all_to_all x1, starting transfers between devices, on_device(): part = lax.all_to_all(part, ('z', 'c', 'yq'), 0, 0, tiled=True)  15.7 us
    all_to_all x1, blocking collectives, on_device(): part = lax.all_to_all(part, ('yp', 'x'), 0, 0, tiled=True)  13.5 us
    all_gather x1, blocking collectives, on_device(): lax.all_gather(arrived.reshape(spots, quarter), 'x', axis=0, tiled=False)  13.3 us
    pallas_call x1, Pallas kernels, on_device(): local(expert_kernel, 'expert', [VMEM] * 4, pltpu.VMEM((2 * X, quads, coun...  2.29 us
  transfers between devices with their start and end apart: 1, of which 1 were waited for; matrix products, arithmetic and copies ran while one was open for 0% of the time, Pallas kernels for 0%

profile of v7, /device:TPU:1, one launch (start us, length us, event | category | flops | bytes accessed | tf_op | source)
XLA Modules:
  0.0 97.2 jit_solution(15582702014302668651)
XLA Ops:
  0.0 0.0 copy-start.1
  0.0 0.0 copy-start.2
  0.0 1.4 %place.1 = bf16[192,640]{1,0:T(8,128)(2,1)S(1)} custom-call(bf16[32,2560]{1,0:T(8,128)(2,1)} %refs_0_.1, f32[2560]{0:T(1024)} %refs_1_.1, s32[4,32]{1,0:T(4,128)} %bitcast.14), custom_call_target="tpu_custom_call" | custom-call | flops 10000000000 | bytes 1000000 | tf_op jit(solution)/shard_map/place/pallas_call | solution.py:170
  1.4 0.0 copy-start
  1.5 31.5 %all_to_all.15 = bf16[24,8,640]{2,1,0:T(8,128)(2,1)S(1)} all-to-all(bf16[24,8,640]{2,1,0:T(8,128)(2,1)S(1)} %bitcast.13), channel_id=1, replica_groups=mesh['z'=12,'c'=2,'yq'=4,'yp'=2,'x'=4] {'z','c'}, dimensions={0} | all-to-all | bytes 491520 | tf_op jit(solution)/shard_map/all_to_all | solution.py:186
  33.0 13.3 %all_gather.3.rows_ref = bf16[4,192,640]{2,1,0:T(8,128)(2,1)S(1)} all-gather(bf16[1,192,640]{2,1,0:T(8,128)(2,1)S(1)} %bitcast.17), channel_id=1, replica_groups=mesh['z'=12,'c'=2,'yq'=4,'yp'=2,'x'=4] {'x'}, dimensions={0}, use_global_device_ids=true | all-gather | bytes 1228800 | tf_op jit(solution)/shard_map/all_gather | solution.py:187
  46.3 0.0 copy-done.1
  46.3 0.0 copy-done.2
  46.3 0.0 copy-done
  46.3 2.3 %expert.1 = bf16[8,4,120,128]{3,2,1,0:T(8,128)(2,1)S(1)} custom-call(bf16[4,192,640]{2,1,0:T(8,128)(2,1)S(1)} %all_gather.3.rows_ref, bf16[280,2560]{1,0:T(8,128)(2,1)S(1)} %bitcast.9, bf16[280,2560]{1,0:T(8,128)(2,1)S(1)} %bitcast.10, bf16[280,2560]{1,0:T(8,128)(2,1)S(1)} %bitcast.11), custom_call_target="tpu_custom_call" | custom-call | tf_op jit(solution)/shard_map/expert/pallas_call | solution.py:190
  48.6 0.0 copy-start.3
  48.6 0.0 copy-start.4
  48.6 13.5 %all_to_all.16.in_ref = bf16[8,4,120,128]{3,2,1,0:T(8,128)(2,1)S(1)} all-to-all(bf16[8,4,120,128]{3,2,1,0:T(8,128)(2,1)S(1)} %expert.1), channel_id=1, replica_groups=mesh['z'=12,'c'=2,'yq'=4,'yp'=2,'x'=4] {'yp','x'}, dimensions={0} | all-to-all | bytes 1966080 | tf_op jit(solution)/shard_map/all_to_all | solution.py:193
  62.1 0.9 sum_x.1
  63.0 15.7 %all-to-all-start.2 = ((bf16[96,8,80]{2,1,0:T(8,128)(2,1)}), bf16[96,8,80]{2,1,0:T(8,128)(2,1)S(1)}, u32[]{:S(2)}, u32[]{:S(2)}) async-start(bf16[96,8,80]{2,1,0:T(8,128)(2,1)} %bitcast.6), calls=%async_computation.2 | async-start | bytes 393216 | tf_op jit(solution)/shard_map/all_to_all | solution.py:198
  78.7 0.0 copy-done.3
  78.7 0.0 copy-done.4
  78.7 0.2 weigh.1.chosen_ref
  78.9 17.5 %all-to-all-done.2 = bf16[96,8,80]{2,1,0:T(8,128)(2,1)S(1)} async-done(((bf16[96,8,80]{2,1,0:T(8,128)(2,1)}), bf16[96,8,80]{2,1,0:T(8,128)(2,1)S(1)}, u32[]{:S(2)}, u32[]{:S(2)}) %all-to-all-start.2) | async-done | bytes 122912 | tf_op jit(solution)/shard_map/all_to_all | solution.py:198
  96.4 0.8 mix.1
Async XLA Ops:
  0.0 46.3 %copy-start.1 = (bf16[1,280,2560]{2,1,0:T(8,128)(2,1)S(1)}, bf16[1,280,2560]{2,1,0:T(8,128)(2,1)}, u32[]{:S(2)}) copy-start(bf16[1,280,2560]{2,1,0:T(8,128)(2,1)} %param.12) | copy-start | bytes 4300804
  0.0 46.3 %copy-start.2 = (bf16[1,280,2560]{2,1,0:T(8,128)(2,1)S(1)}, bf16[1,280,2560]{2,1,0:T(8,128)(2,1)}, u32[]{:S(2)}) copy-start(bf16[1,280,2560]{2,1,0:T(8,128)(2,1)} %param.13) | copy-start | bytes 4300804
  1.4 44.9 %copy-start = (bf16[1,280,2560]{2,1,0:T(8,128)(2,1)S(1)}, bf16[1,280,2560]{2,1,0:T(8,128)(2,1)}, u32[]{:S(2)}) copy-start(bf16[1,280,2560]{2,1,0:T(8,128)(2,1)} %param.11) | copy-start | bytes 4300804
  48.6 30.1 %copy-start.3 = (s32[32,4]{0,1:T(4,128)S(1)}, s32[32,4]{0,1:T(4,128)}, u32[]{:S(2)}) copy-start(s32[32,4]{0,1:T(4,128)} %param.9) | copy-start | bytes 1540
  48.6 30.1 %copy-start.4 = (f32[32,4]{0,1:T(4,128)S(1)}, f32[32,4]{0,1:T(4,128)}, u32[]{:S(2)}) copy-start(f32[32,4]{0,1:T(4,128)} %param.10) | copy-start | bytes 1540
  63.0 33.4 %all-to-all-start.2 = ((bf16[96,8,80]{2,1,0:T(8,128)(2,1)}), bf16[96,8,80]{2,1,0:T(8,128)(2,1)S(1)}, u32[]{:S(2)}, u32[]{:S(2)}) async-start(bf16[96,8,80]{2,1,0:T(8,128)(2,1)} %bitcast.6), calls=%async_computation.2 | async-start | bytes 393216 | tf_op jit(solution)/shard_map/all_to_all | solution.py:198

commit v8 on v6

--- a/solution.py
+++ b/solution.py
@@ -63,7 +63,7 @@
         pltpu.make_async_copy(source, there, sems.at[i])
         for i, (source, there) in enumerate(zip(sources, refs[6:10]))
     ]
-    for i in (2, 3, 0, 1):
+    for i in (0, 2, 3, 1):
         copies[i].start()
     rows = tokens_ref.shape[0]
     share = send_ref.shape[1]

time: 96.4 us -> 96.4 us (level)
  no operation moved by 1% of the time
where the time goes in v8:
time: 96.4 us; the launch traced here: 96.2 us
  blocking collectives  91.4 us (95%)
  Pallas kernels  4.78 us (5%)
    all_to_all x1, blocking collectives, on_device(): part = lax.all_to_all(part, ('z', 'c', 'yq'), 0, 0, tiled=True)  33.2 us
    all_to_all x1, blocking collectives, on_device(): lax.all_to_all(send.reshape(EP, CAP, quarter), ep, 0, 0, tiled=True)  31.5 us
    all_to_all x1, blocking collectives, on_device(): part = lax.all_to_all(part, ('yp', 'x'), 0, 0, tiled=True)  13.3 us
    all_gather x1, blocking collectives, on_device(): lax.all_gather(arrived.reshape(spots, quarter), 'x', axis=0, tiled=False)  13.3 us
    pallas_call x1, Pallas kernels, on_device(): local(expert_kernel, 'expert', [VMEM] * 4, pltpu.VMEM((2 * X, quads, coun...  2.29 us

profile of v8, /device:TPU:1, one launch (start us, length us, event | category | flops | bytes accessed | tf_op | source)
XLA Modules:
  0.0 96.2 jit_solution(3341804943070472419)
XLA Ops:
  0.0 0.0 copy-start.1
  0.0 0.0 copy-start.2
  0.0 1.5 %place.1 = (bf16[192,640]{1,0:T(8,128)(2,1)S(1)}, bf16[3,32,192]{2,1,0:T(8,128)(2,1)S(1)}) custom-call(bf16[32,2560]{1,0:T(8,128)(2,1)} %refs_0_.1, f32[2560]{0:T(1024)} %refs_1_.1, s32[4,32]{1,0:T(4,128)} %bitcast.16, f32[4,32]{1,0:T(4,128)} %bitcast.17), custom_call_target="tpu_custom_call" | custom-call | flops 10000000000 | bytes 1000000 | tf_op jit(solution)/shard_map/place/pallas_call | solution.py:162
  1.5 0.0 copy-start
  1.5 31.5 %all_to_all.15 = bf16[24,8,640]{2,1,0:T(8,128)(2,1)S(1)} all-to-all(bf16[24,8,640]{2,1,0:T(8,128)(2,1)S(1)} %bitcast.14), channel_id=1, replica_groups=mesh['z'=12,'c'=2,'yq'=4,'yp'=2,'x'=4] {'z','c'}, dimensions={0} | all-to-all | bytes 491520 | tf_op jit(solution)/shard_map/all_to_all | solution.py:171
  33.0 13.3 %all_gather.3.rows_ref = bf16[4,192,640]{2,1,0:T(8,128)(2,1)S(1)} all-gather(bf16[1,192,640]{2,1,0:T(8,128)(2,1)S(1)} %bitcast.15), channel_id=1, replica_groups=mesh['z'=12,'c'=2,'yq'=4,'yp'=2,'x'=4] {'x'}, dimensions={0}, use_global_device_ids=true | all-gather | bytes 1228800 | tf_op jit(solution)/shard_map/all_gather | solution.py:172
  46.4 0.0 copy-done.1
  46.4 0.0 copy-done.2
  46.4 0.0 copy-done
  46.4 2.3 %expert.1 = bf16[8,4,120,128]{3,2,1,0:T(8,128)(2,1)S(1)} custom-call(bf16[4,192,640]{2,1,0:T(8,128)(2,1)S(1)} %all_gather.3.rows_ref, bf16[280,2560]{1,0:T(8,128)(2,1)S(1)} %bitcast.9, bf16[280,2560]{1,0:T(8,128)(2,1)S(1)} %bitcast.10, bf16[280,2560]{1,0:T(8,128)(2,1)S(1)} %bitcast.11), custom_call_target="tpu_custom_call" | custom-call | tf_op jit(solution)/shard_map/expert/pallas_call | solution.py:175
  48.7 13.3 %all_to_all.16.in_ref = bf16[8,4,120,128]{3,2,1,0:T(8,128)(2,1)S(1)} all-to-all(bf16[8,4,120,128]{3,2,1,0:T(8,128)(2,1)S(1)} %expert.1), channel_id=1, replica_groups=mesh['z'=12,'c'=2,'yq'=4,'yp'=2,'x'=4] {'yp','x'}, dimensions={0} | all-to-all | bytes 1966080 | tf_op jit(solution)/shard_map/all_to_all | solution.py:178
  62.0 0.2 sum_x.1
  62.3 33.2 %all_to_all.17 = bf16[96,8,80]{2,1,0:T(8,128)(2,1)S(1)} all-to-all(bf16[96,8,80]{2,1,0:T(8,128)(2,1)S(1)} %bitcast.12), channel_id=1, replica_groups=mesh['z'=12,'c'=2,'yq'=4,'yp'=2,'x'=4] {'z','c','yq'}, dimensions={0} | all-to-all | bytes 245760 | tf_op jit(solution)/shard_map/all_to_all | solution.py:183
  95.4 0.8 mix.1
Async XLA Ops:
  0.0 46.4 %copy-start.1 = (bf16[1,280,2560]{2,1,0:T(8,128)(2,1)S(1)}, bf16[1,280,2560]{2,1,0:T(8,128)(2,1)}, u32[]{:S(2)}) copy-start(bf16[1,280,2560]{2,1,0:T(8,128)(2,1)} %param.12) | copy-start | bytes 4300804
  0.0 46.4 %copy-start.2 = (bf16[1,280,2560]{2,1,0:T(8,128)(2,1)S(1)}, bf16[1,280,2560]{2,1,0:T(8,128)(2,1)}, u32[]{:S(2)}) copy-start(bf16[1,280,2560]{2,1,0:T(8,128)(2,1)} %param.13) | copy-start | bytes 4300804
  1.5 44.9 %copy-start = (bf16[1,280,2560]{2,1,0:T(8,128)(2,1)S(1)}, bf16[1,280,2560]{2,1,0:T(8,128)(2,1)}, u32[]{:S(2)}) copy-start(bf16[1,280,2560]{2,1,0:T(8,128)(2,1)} %param.11) | copy-start | bytes 4300804
